TPU v7x, 512 devices: a whole 4x8x8 slice. The times are simulated.
512 devices in a mesh: sp: 64 (over z, y), fs: 4 (over x), tp: 2 (over core).
Axes of the slice: x: 4, y: 8, z: 8, core: 2. Of those that a mesh axis runs over, the one named last changes fastest.
Arguments:
- output_gate_logits: bfloat16 [4, 8192, 2048], P('fs', 'sp', 'tp'), may hold values from -6 to 6
- head_input_rows: bfloat16 [4, 8192, 2048], P('fs', 'sp', 'tp'), may hold values from -6 to 6
- group_state_writes: bfloat16 [4, 8192, 512], P('fs', 'sp', 'tp'), may hold values from -6 to 6
- group_state_reads: bfloat16 [4, 8192, 512], P('fs', 'sp', 'tp'), may hold values from -6 to 6
- step_logits: float32 [4, 8192, 32], P('fs', 'sp', 'tp'), may hold values from -5 to 5
- head_step_offset: float32 [32], P('tp'), may hold values from -3.5 to 1
- head_decay_logrates: float32 [32], P('tp'), may hold values from -11 to 0
- decay_extra_spikes: float32 [8192, 32], P('sp', 'tp'), may hold values from -2.1 to 0
- head_input_taps: bfloat16 [4, 2048], P(None, 'tp'), may hold values from -3 to 3
- state_input_taps: bfloat16 [4, 512], P(None, 'tp'), may hold values from -3 to 3
- readout_filter_taps: bfloat16 [4, 512], P(None, 'tp'), may hold values from -3 to 3
- grouped_norm_scale: float32 [2048], P('tp'), may hold values from 0.1 to 1.9
- convolution_outer_gate: bfloat16 [4, 8192, 1024], P('fs', 'sp', 'tp'), may hold values from -6 to 6
- convolution_inner_gate: bfloat16 [4, 8192, 1024], P('fs', 'sp', 'tp'), may hold values from -6 to 6
- convolution_value_rows: bfloat16 [4, 8192, 1024], P('fs', 'sp', 'tp'), may hold values from -6 to 6
- gated_filter_taps: bfloat16 [3, 1024], P(None, 'tp'), may hold values from -3.5 to 3.5
- state_output_rows: bfloat16 [2048, 2048], P('tp', 'fs'), may hold values from -0.09375 to 0.09375
- convolution_output_rows: bfloat16 [1024, 2048], P('tp', 'fs'), may hold values from -0.125 to 0.125
Outputs:
- layer_out: bfloat16 [4, 8192, 2048], P('tp', 'sp', 'fs')
All inputs are finite; a program needn't handle non-finite values.
Results may differ from a plain program's by a relative error of at most 0.012.
Values may be sent and summed in bfloat16 or wider, within the bound.
No kernel may reach another device: no remote copies, remote signals or barrier semaphores. Data moves between devices by JAX's collectives and lax.ppermute only.
A program may use at most 64 MiB of HBM per device.

v0:
```python
import jax
import jax.numpy as jnp
from jax import lax
from jax.sharding import PartitionSpec as P

STATE = 128
BLOCK = 128


EPS = 1e-06
HIGH = lax.Precision.HIGHEST


def shifted(value, axis, steps):
    count = lax.axis_size(axis)
    first, last = (max(0, -steps), min(count, count - steps))
    return lax.ppermute(value, axis, [(source, source + steps) for source in range(first, last)])


def cut_along(array, dim, size):
    lengths = array.shape
    pieces = array.reshape(*lengths[:dim], size, lengths[dim] // size, *lengths[dim + 1 :])
    return jnp.moveaxis(pieces, dim, 0)


def edges_of(length, count):
    turn = length // count
    if turn >= 8:
        turn -= turn % 8
    return [turn * k for k in range(1, count)]


def in_order(pieces, dim):
    lengths = list(pieces.shape[1:])
    lengths[dim] *= pieces.shape[0]
    return jnp.moveaxis(pieces, 0, dim).reshape(lengths)


def several_exchanges(array, axis, pieces, split_dim, concat_dim):
    blocks = cut_along(array, split_dim, lax.axis_size(axis))
    cut = max(range(1, max(2, blocks.ndim - 1)), key=lambda d: blocks.shape[d])
    gathered = []
    for piece in jnp.split(blocks, edges_of(blocks.shape[cut], pieces), axis=cut):
        if piece.size:
            gathered.append(lax.all_to_all(piece, axis, split_axis=0, concat_axis=0, tiled=True))
    return in_order(jnp.concatenate(gathered, axis=cut), concat_dim)


def from_everyone(array, axis):
    size = lax.axis_size(axis)
    return lax.all_to_all(
        jnp.broadcast_to(array[None], (size, *array.shape)), axis, 0, 0, tiled=True
    )


def gather_directly(array, axis, dim):
    return in_order(from_everyone(array, axis), dim)


def summed_on_arrival(array, axis, dim):
    size = lax.axis_size(axis)
    pieces = lax.all_to_all(cut_along(array, dim, size), axis, 0, 0, tiled=True)
    return jnp.sum(pieces.astype(jnp.float32), axis=0)


def causal_filter(stream, kernel, before):
    span = kernel.shape[0]
    length = stream.shape[1]
    padded = jnp.concatenate([before, stream], axis=1)
    total = padded[:, 0:length] * kernel[0]
    for offset in range(1, span):
        total = total + padded[:, offset : offset + length] * kernel[offset]
    return total


def block_scan(driven, decay, writes, reads):
    batch, length, groups, ratio, channels = driven.shape
    entries = writes.shape[-1]
    count = length // BLOCK

    def split(array):
        shaped = array.reshape((batch, count, BLOCK) + array.shape[2:])
        return jnp.moveaxis(shaped, 1, 0)

    causal = jnp.tril(jnp.ones((BLOCK, BLOCK), dtype=bool))

    def advance(carry, pieces):
        drive, fall, write, read = pieces
        rising = jnp.cumsum(fall, axis=1)
        scores = jnp.einsum("blgn,bsgn->bgls", read, write, precision=HIGH)
        gaps = rising[:, :, None] - rising[:, None, :]
        weights = jnp.exp(jnp.where(causal[None, :, :, None, None], gaps, -jnp.inf))
        inside = jnp.einsum("bgls,blsgr,bsgrp->blgrp", scores, weights, drive, precision=HIGH)
        earlier = (
            jnp.einsum("blgn,bgrpn->blgrp", read, carry, precision=HIGH)
            * jnp.exp(rising)[..., None]
        )
        remain = jnp.exp(rising[:, -1:] - rising)
        fresh = jnp.einsum("bsgn,bsgr,bsgrp->bgrpn", write, remain, drive, precision=HIGH)
        carry = carry * jnp.exp(rising[:, -1])[..., None, None] + fresh
        return (carry, inside + earlier)

    start = jnp.zeros((batch, groups, ratio, channels, entries), jnp.float32)
    final, blocks = lax.scan(
        advance, start, (split(driven), split(decay), split(writes), split(reads))
    )
    return (final, jnp.moveaxis(blocks, 0, 1).reshape(driven.shape))


def per_device(
    output_gate_logits,
    head_input_rows,
    group_state_writes,
    group_state_reads,
    step_logits,
    head_step_offset,
    head_decay_logrates,
    decay_extra_spikes,
    head_input_taps,
    state_input_taps,
    readout_filter_taps,
    grouped_norm_scale,
    convolution_outer_gate,
    convolution_inner_gate,
    convolution_value_rows,
    gated_filter_taps,
    state_output_rows,
    convolution_output_rows,
):
    batch, length, head_width = head_input_rows.shape
    heads = step_logits.shape[2]
    group_width = group_state_writes.shape[2]
    groups = group_width // STATE
    ratio = heads // groups
    channels = head_width // heads
    conv_width = convolution_inner_gate.shape[2]
    reach = head_input_taps.shape[0] - 1
    short = gated_filter_taps.shape[0] - 1
    rims = jnp.concatenate(
        [
            head_input_rows[:, -reach:],
            group_state_writes[:, -reach:],
            group_state_reads[:, -reach:],
            convolution_inner_gate[:, -reach:],
            convolution_value_rows[:, -reach:],
        ],
        axis=2,
    )
    before = shifted(rims, "sp", 1).astype(jnp.float32)
    second = head_width + group_width
    third = second + group_width
    fourth = third + conv_width
    before_input = before[:, :, :head_width]
    before_writes = before[:, :, head_width:second]
    before_reads = before[:, :, second:third]
    before_inner = before[:, reach - short :, third:fourth]
    before_values = before[:, reach - short :, fourth:]
    product = convolution_inner_gate.astype(jnp.float32) * convolution_value_rows.astype(
        jnp.float32
    )
    filtered = causal_filter(
        product, gated_filter_taps.astype(jnp.float32), before_inner * before_values
    )
    conv_branch = (convolution_outer_gate.astype(jnp.float32) * filtered).astype(jnp.bfloat16)
    conv_rows = conv_branch.reshape(batch * length, conv_width)

    def project_conv(piece):
        return jnp.dot(piece, convolution_output_rows, preferred_element_type=jnp.float32)

    filtered_input = jax.nn.silu(
        causal_filter(
            head_input_rows.astype(jnp.float32), head_input_taps.astype(jnp.float32), before_input
        )
    )
    filtered_writes = jax.nn.silu(
        causal_filter(
            group_state_writes.astype(jnp.float32),
            state_input_taps.astype(jnp.float32),
            before_writes,
        )
    )
    filtered_reads = jax.nn.silu(
        causal_filter(
            group_state_reads.astype(jnp.float32),
            readout_filter_taps.astype(jnp.float32),
            before_reads,
        )
    )
    head_step_length = jax.nn.softplus(step_logits + head_step_offset)
    decay_logarithm = decay_extra_spikes[None] - head_step_length * jnp.exp(head_decay_logrates)
    driven = (
        filtered_input.reshape(batch, length, heads, channels) * head_step_length[..., None]
    ).reshape(batch, length, groups, ratio, channels)
    decay_grouped = decay_logarithm.reshape(batch, length, groups, ratio)
    reads_grouped = filtered_reads.reshape(batch, length, groups, STATE)
    final, inside = block_scan(
        driven, decay_grouped, filtered_writes.reshape(batch, length, groups, STATE), reads_grouped
    )
    totals = jnp.sum(decay_grouped, axis=1)
    flattened = final.reshape(batch, groups, ratio, channels * STATE)[None]
    slices = several_exchanges(flattened.astype(jnp.bfloat16), "sp", 2, 4, 0).astype(
        flattened.dtype
    )
    every_total = gather_directly(totals[None], "sp", 0)
    through = jnp.cumsum(every_total, axis=0)
    before_total = through - every_total
    members = every_total.shape[0]
    earlier_mask = jnp.arange(members)[:, None] > jnp.arange(members)[None, :]
    log_gaps = before_total[:, None] - through[None, :]
    weights = jnp.where(
        earlier_mask[:, :, None, None, None], jnp.exp(jnp.minimum(log_gaps, 0.0)), 0.0
    )
    prefixes = jnp.einsum("jibgr,ibgre->jbgre", weights, slices, precision=HIGH)
    incoming = (
        lax.all_to_all(prefixes.astype(jnp.bfloat16), "sp", split_axis=0, concat_axis=4, tiled=True)
        .astype(prefixes.dtype)[0]
        .reshape(final.shape)
    )
    rising = jnp.cumsum(decay_grouped, axis=1)
    carried = (
        jnp.einsum("blgn,bgrpn->blgrp", reads_grouped, incoming, precision=HIGH)
        * jnp.exp(rising)[..., None]
    )
    state_output = (inside + carried).reshape(batch, length, head_width)
    gated = state_output * jax.nn.silu(output_gate_logits.astype(jnp.float32))
    grouped = gated.reshape(batch, length, groups, ratio * channels)
    normed = grouped * lax.rsqrt(jnp.mean(grouped * grouped, axis=-1, keepdims=True) + EPS)
    state_branch = (normed.reshape(batch, length, head_width) * grouped_norm_scale).astype(
        jnp.bfloat16
    )
    state_rows = state_branch.reshape(batch * length, head_width)
    joined = jnp.concatenate([state_rows, conv_rows], axis=1)
    piece = gather_directly(joined, "fs", 0)
    project_piece = piece[:, :head_width]
    terms = jnp.dot(
        project_piece, state_output_rows, preferred_element_type=jnp.float32
    ) + project_conv(piece[:, head_width:])
    summed = summed_on_arrival(terms.astype(jnp.bfloat16), "tp", 0)
    return summed.astype(jnp.bfloat16).reshape(-1, length, summed.shape[1])


def solution(mesh):
    return jax.shard_map(
        per_device,
        mesh=mesh,
        in_specs=(
            P("fs", "sp", "tp"),
            P("fs", "sp", "tp"),
            P("fs", "sp", "tp"),
            P("fs", "sp", "tp"),
            P("fs", "sp", "tp"),
            P("tp"),
            P("tp"),
            P("sp", "tp"),
            P(None, "tp"),
            P(None, "tp"),
            P(None, "tp"),
            P("tp"),
            P("fs", "sp", "tp"),
            P("fs", "sp", "tp"),
            P("fs", "sp", "tp"),
            P(None, "tp"),
            P("tp", "fs"),
            P("tp", "fs"),
        ),
        out_specs=P("tp", "sp", "fs"),
        check_vma=False,
    )
```

profile of v0, /device:TPU:1, one launch (start us, length us, event | category | flops | bytes accessed | tf_op | source)
XLA Modules:
  0.0 130.9 jit_solution(876774140327506008)
XLA Ops:
  0.0 0.8 constant_dynamic-update-slice_fusion.4
  0.9 0.7 constant_dynamic-update-slice_fusion.3
  1.6 0.7 constant_dynamic-update-slice_fusion.2
  2.3 0.7 constant_dynamic-update-slice_fusion.1
  3.0 0.7 constant_dynamic-update-slice_fusion
  3.7 4.0 %collective-permute-start = (bf16[1,3,2560]{2,1,0:T(4,128)(2,1)S(1)}, bf16[1,3,2560]{2,1,0:T(4,128)(2,1)S(1)}, u32[]{:S(2)}, u32[]{:S(2)}) collective-permute-start(bf16[1,3,2560]{2,1,0:T(4,128)(2,1)S(1)} %constant_dynamic-update-slice_fusion), channel_id=1, source_target_pairs={{0,8},{8,16},{16,24},{24,32},{32,40},{40,48},{48,56},{56,64},{64,7... | collective-permute-start | bytes 46088 | tf_op jit(solution)/shard_map/ppermute | solution.py:17
  8.3 0.9 fusion.91
  10.0 15.4 %all-to-all-start.2 = ((f32[64,1,1,2,8]{4,3,2,1,0:T(2,128)}), f32[64,1,1,2,8]{4,3,2,1,0:T(2,128)S(1)}, u32[]{:S(2)}, u32[]{:S(2)}) async-start(f32[64,1,1,2,8]{4,3,2,1,0:T(2,128)} %broadcast_in_dim.82), calls=%async_computation.2 | async-start | bytes 131072 | tf_op jit(solution)/shard_map/all_to_all | solution.py:51
  26.3 1.0 copy.86
  27.3 1.0 copy.87
  28.4 0.8 fusion.97
  29.2 0.8 fusion.96
  30.0 0.8 fusion.95
  30.8 0.9 fusion.94
  32.6 0.8 divide_multiply_fusion.1
  33.7 1.4 %divide_multiply_fusion = f32[1,128,1024]{1,2,0:T(8,128)S(1)} fusion(f32[1,128,1024]{1,2,0:T(8,128)S(1)} %convert_element_type.74, f32[1,3,1024]{1,2,0:T(8,128)S(1)} %copy.66, f32[1024]{0:T(1024)S(1)} %bitcast.127, f32[1024]{0:T(1024)S(1)} %bitcast.126, f32[1024]{0:T(1024)S(1)} %bitcast.125, f32[1024]{0:T(1024)S(1)} %bitcast.124), kind=kLoop, calls=%fused_computation.51 | loop fusion | flops 1835008 | bytes 1077248 | tf_op jit(solution)/shard_map/jit(silu)/mul | solution.py:170
  35.2 1.3 %fusion.7 = bf16[64,1,1,2,8,128]{5,0,4,3,2,1:T(8,128)(2,1)S(1)} fusion(f32[128,2,8,64]{0,3,2,1:T(8,128)S(1)} %bitcast.110, f32[128,2,8]{0,2,1:T(8,128)S(1)} %copy.69, f32[2,8]{1,0:T(2,128)} %exponential_multiply_fusion, f32[128,2,8]{0,2,1:T(8,128)S(1)} %get-tuple-element.37, f32[128,2,128,1]{2,1,0,3:T(2,128)S(1)} %bitcast.119), kind=kOutput, calls=%fused_computation.17 | convolution fusion | flops 201850880 | bytes 933952 | tf_op jit(solution)/shard_map/while/body/eval_jaxpr/bsgn,bsgr,bsgrp->bgrpn/dot_general | solution.py:99
  36.6 0.7 copy.71
  37.3 12.1 %all-to-all-start = ((bf16[64,1,1,2,4,128]{5,4,3,2,1,0:T(4,128)(2,1)}), bf16[64,1,1,2,4,128]{5,4,3,2,1,0:T(4,128)(2,1)S(1)}, u32[]{:S(2)}, u32[]{:S(2)}) async-start(bf16[64,1,1,2,4,128]{5,4,3,2,1,0:T(4,128)(2,1)} %copy.71), calls=%async_computation | async-start | bytes 262144 | tf_op jit(solution)/shard_map/all_to_all | solution.py:45
  50.5 1.1 copy.84
  51.7 0.8 copy.72
  52.5 8.6 %all-to-all-done = bf16[64,1,1,2,4,128]{5,4,3,2,1,0:T(4,128)(2,1)S(1)} async-done(((bf16[64,1,1,2,4,128]{5,4,3,2,1,0:T(4,128)(2,1)}), bf16[64,1,1,2,4,128]{5,4,3,2,1,0:T(4,128)(2,1)S(1)}, u32[]{:S(2)}, u32[]{:S(2)}) %all-to-all-start) | async-done | bytes 131104 | tf_op jit(solution)/shard_map/all_to_all | solution.py:45
  61.0 4.6 %all-to-all-start.1 = ((bf16[64,1,1,2,4,128]{5,4,3,2,1,0:T(4,128)(2,1)}), bf16[64,1,1,2,4,128]{5,4,3,2,1,0:T(4,128)(2,1)S(1)}, u32[]{:S(2)}, u32[]{:S(2)}) async-start(bf16[64,1,1,2,4,128]{5,4,3,2,1,0:T(4,128)(2,1)} %copy.72), calls=%async_computation.1 | async-start | bytes 262144 | tf_op jit(solution)/shard_map/all_to_all | solution.py:45
  66.4 10.9 %all-to-all-done.1 = bf16[64,1,1,2,4,128]{5,4,3,2,1,0:T(4,128)(2,1)S(1)} async-done(((bf16[64,1,1,2,4,128]{5,4,3,2,1,0:T(4,128)(2,1)}), bf16[64,1,1,2,4,128]{5,4,3,2,1,0:T(4,128)(2,1)S(1)}, u32[]{:S(2)}, u32[]{:S(2)}) %all-to-all-start.1) | async-done | bytes 131104 | tf_op jit(solution)/shard_map/all_to_all | solution.py:45
  77.8 0.9 copy.79
  78.7 4.8 %all-to-all-start.3 = ((bf16[64,1,2,8,128]{4,3,2,1,0:T(8,128)(2,1)}), bf16[64,1,2,8,128]{4,3,2,1,0:T(8,128)(2,1)S(1)}, u32[]{:S(2)}, u32[]{:S(2)}) async-start(bf16[64,1,2,8,128]{4,3,2,1,0:T(8,128)(2,1)} %copy.79), calls=%async_computation.3 | async-start | bytes 524288 | tf_op jit(solution)/shard_map/all_to_all | solution.py:215
  84.7 11.1 %all-to-all-done.3 = bf16[64,1,2,8,128]{4,3,2,1,0:T(8,128)(2,1)S(1)} async-done(((bf16[64,1,2,8,128]{4,3,2,1,0:T(8,128)(2,1)}), bf16[64,1,2,8,128]{4,3,2,1,0:T(8,128)(2,1)S(1)}, u32[]{:S(2)}, u32[]{:S(2)}) %all-to-all-start.3) | async-done | bytes 262176 | tf_op jit(solution)/shard_map/all_to_all | solution.py:215
  96.3 2.3 %fusion.2 = f32[1,128,2,8,64]{1,4,3,2,0:T(8,128)S(1)} fusion(f32[1,128,2,8,64]{1,4,3,2,0:T(8,128)S(1)} %fusion.4, f32[1,128,2,8,64]{1,4,3,2,0:T(8,128)S(1)} %fusion.3, f32[128,2,8]{0,2,1:T(8,128)S(1)} %copy.63, f32[128,128,2]{1,0,2:T(8,128)S(1)} %convolution_bitcast_fusion.3, pred[128,128]{1,0:T(8,128)(4,1)S(1)} %iota_compare_fusion, ...), kind=kOutput, calls=%fused_computation.11 | convolution fusion | flops 202506240 | bytes 2260992 | tf_op jit(solution)/shard_map/while/body/eval_jaxpr/bgls,blsgr,bsgrp->blgrp/dot_general | solution.py:93
  99.3 19.2 %all_to_all.40 = bf16[4,128,1536]{2,1,0:T(8,128)(2,1)S(1)} all-to-all(bf16[4,128,1536]{2,1,0:T(8,128)(2,1)S(1)} %broadcast_in_dim.83), channel_id=1, replica_groups=mesh['sp'=64,'fs'=4,'tp'=2] {'fs'}, dimensions={0} | all-to-all | bytes 3145728 | tf_op jit(solution)/shard_map/all_to_all | solution.py:51
  118.6 0.7 fusion.8
  120.1 10.0 %all_to_all.41 = bf16[2,256,512]{2,1,0:T(8,128)(2,1)S(1)} all-to-all(bf16[2,256,512]{2,1,0:T(8,128)(2,1)S(1)} %bitcast.114), channel_id=1, replica_groups=mesh['sp'=64,'fs'=4,'tp'=2] {'tp'}, dimensions={0} | all-to-all | bytes 1048576 | tf_op jit(solution)/shard_map/all_to_all | solution.py:62
  130.1 0.8 reduce_sum.32
  (71 shorter events, 8.8 us)
Async XLA Ops:
  0.0 118.6 %copy-start = (bf16[1024,512]{1,0:T(8,128)(2,1)S(1)}, bf16[1024,512]{1,0:T(8,128)(2,1)}, u32[]{:S(2)}) copy-start(bf16[1024,512]{1,0:T(8,128)(2,1)} %param.34) | copy-start | bytes 3145732
  0.0 32.3 %copy-start.3 = (bf16[1,128,1024]{2,1,0:T(8,128)(2,1)S(1)}, bf16[1,128,1024]{2,1,0:T(8,128)(2,1)}, u32[]{:S(2)}) copy-start(bf16[1,128,1024]{2,1,0:T(8,128)(2,1)} %param.19) | copy-start | bytes 786436
  0.0 32.2 %copy-start.5 = (bf16[1,128,256]{2,1,0:T(8,128)(2,1)S(1)}, bf16[1,128,256]{2,1,0:T(8,128)(2,1)}, u32[]{:S(2)}) copy-start(bf16[1,128,256]{2,1,0:T(8,128)(2,1)} %param.20) | copy-start | bytes 196612
  0.0 32.2 %copy-start.6 = (bf16[1,128,256]{2,1,0:T(8,128)(2,1)S(1)}, bf16[1,128,256]{2,1,0:T(8,128)(2,1)}, u32[]{:S(2)}) copy-start(bf16[1,128,256]{2,1,0:T(8,128)(2,1)} %param.21) | copy-start | bytes 196612
  3.7 28.9 %collective-permute-start = (bf16[1,3,2560]{2,1,0:T(4,128)(2,1)S(1)}, bf16[1,3,2560]{2,1,0:T(4,128)(2,1)S(1)}, u32[]{:S(2)}, u32[]{:S(2)}) collective-permute-start(bf16[1,3,2560]{2,1,0:T(4,128)(2,1)S(1)} %constant_dynamic-update-slice_fusion), channel_id=1, source_target_pairs={{0,8},{8,16},{16,24},{24,32},{32,40},{40,48},{48,56},{56,64},{64,7... | collective-permute-start | bytes 46088 | tf_op jit(solution)/shard_map/ppermute | solution.py:17
  10.0 27.3 %all-to-all-start.2 = ((f32[64,1,1,2,8]{4,3,2,1,0:T(2,128)}), f32[64,1,1,2,8]{4,3,2,1,0:T(2,128)S(1)}, u32[]{:S(2)}, u32[]{:S(2)}) async-start(f32[64,1,1,2,8]{4,3,2,1,0:T(2,128)} %broadcast_in_dim.82), calls=%async_computation.2 | async-start | bytes 131072 | tf_op jit(solution)/shard_map/all_to_all | solution.py:51
  35.2 15.1 %copy-start.4 = (bf16[1,128,512]{2,1,0:T(8,128)(2,1)S(1)}, bf16[1,128,512]{2,1,0:T(8,128)(2,1)}, u32[]{:S(2)}) copy-start(bf16[1,128,512]{2,1,0:T(8,128)(2,1)} %param.30) | copy-start | bytes 393220
  36.5 29.3 %copy-start.2 = (f32[1,128,256]{2,1,0:T(8,128)S(1)}, f32[1,128,256]{2,1,0:T(8,128)}, u32[]{:S(2)}) copy-start(f32[1,128,256]{2,1,0:T(8,128)} %get-tuple-element.54) | copy-start | bytes 393220
  37.3 23.7 %all-to-all-start = ((bf16[64,1,1,2,4,128]{5,4,3,2,1,0:T(4,128)(2,1)}), bf16[64,1,1,2,4,128]{5,4,3,2,1,0:T(4,128)(2,1)S(1)}, u32[]{:S(2)}, u32[]{:S(2)}) async-start(bf16[64,1,1,2,4,128]{5,4,3,2,1,0:T(4,128)(2,1)} %copy.71), calls=%async_computation | async-start | bytes 262144 | tf_op jit(solution)/shard_map/all_to_all | solution.py:45
  50.3 27.0 %copy-start.7 = (pred[64,64]{1,0:T(8,128)(4,1)S(1)}, pred[64,64]{1,0:T(8,128)(4,1)}, u32[]{:S(2)}) copy-start(pred[64,64]{1,0:T(8,128)(4,1)} %iota_compare_fusion.1) | copy-start | bytes 12292
  61.0 16.2 %all-to-all-start.1 = ((bf16[64,1,1,2,4,128]{5,4,3,2,1,0:T(4,128)(2,1)}), bf16[64,1,1,2,4,128]{5,4,3,2,1,0:T(4,128)(2,1)S(1)}, u32[]{:S(2)}, u32[]{:S(2)}) async-start(bf16[64,1,1,2,4,128]{5,4,3,2,1,0:T(4,128)(2,1)} %copy.72), calls=%async_computation.1 | async-start | bytes 262144 | tf_op jit(solution)/shard_map/all_to_all | solution.py:45
  78.7 17.2 %all-to-all-start.3 = ((bf16[64,1,2,8,128]{4,3,2,1,0:T(8,128)(2,1)}), bf16[64,1,2,8,128]{4,3,2,1,0:T(8,128)(2,1)S(1)}, u32[]{:S(2)}, u32[]{:S(2)}) async-start(bf16[64,1,2,8,128]{4,3,2,1,0:T(8,128)(2,1)} %copy.79), calls=%async_computation.3 | async-start | bytes 524288 | tf_op jit(solution)/shard_map/all_to_all | solution.py:215
  96.2 2.5 %copy-start.8 = (f32[1024]{0:T(1024)S(1)}, f32[1024]{0:T(1024)}, u32[]{:S(2)}) copy-start(f32[1024]{0:T(1024)} %param.29) | copy-start | bytes 12292
  118.6 1.0 copy-start.1
where the time goes:
time: 132 us; the launch traced here: 131 us
  starting transfers between devices  41 us (31%)
  waiting for transfers between devices  30.6 us (23%)
  blocking collectives  29.3 us (22%)
  local copies, waits for them, and re-layouts  16.3 us (12%)
  other arithmetic  6.85 us (5%)
  matrix products  6.58 us (5%)
    all_to_all x2, waiting for transfers between devices, several_exchanges(): lax.all_to_all(piece, axis, split_axis=0, concat_axis=0, tiled=True)  19.4 us
    all_to_all x1, blocking collectives, from_everyone(): lax.all_to_all(jnp.broadcast_to(array[None], (size, *array.shape)), axis,...  19.2 us
    all_to_all x2, starting transfers between devices, several_exchanges(): lax.all_to_all(piece, axis, split_axis=0, concat_axis=0, tiled=True)  16.8 us
    all_to_all x1, starting transfers between devices, from_everyone(): lax.all_to_all(jnp.broadcast_to(array[None], (size, *array.shape)), axis,...  15.4 us
    all_to_all x1, waiting for transfers between devices, per_device(): lax.all_to_all(prefixes.astype(jnp.bfloat16), 'sp', split_axis=0, concat_...  11.1 us
    all_to_all x1, blocking collectives, summed_on_arrival(): pieces = lax.all_to_all(cut_along(array, dim, size), axis, 0, 0, tiled=True)  10 us
    unnamed x27, local copies, waits for them, and re-layouts  6.79 us
    all_to_all x1, starting transfers between devices, per_device(): lax.all_to_all(prefixes.astype(jnp.bfloat16), 'sp', split_axis=0, concat_...  4.8 us
  transfers between devices with their start and end apart: 5, of which 3 were waited for; matrix products, arithmetic and copies ran while one was open for 14% of the time, Pallas kernels for 0%

commit v1 on v0

v1 whole, which is shorter than its diff:
```python
import jax
import jax.numpy as jnp
from jax import lax
from jax.experimental import pallas as pl
from jax.experimental.pallas import tpu as pltpu
from jax.sharding import PartitionSpec as P

EPS = 1e-06
F32 = jnp.float32
BF16 = jnp.bfloat16
STATE = 128
LANES = 128
HEAD_DIM = 64
EXTRA = 8
RIM = 8
HEAD = 16


def whole(shape):
    return pl.BlockSpec(shape, lambda *_: (0,) * len(shape))


HBM = pl.BlockSpec(memory_space=pltpu.HBM)


def call(kernel, outs, ins, far=0, scratch=(), flops=50_000_000):
    ins = [pltpu.with_memory_space_constraint(a, pltpu.HBM) for a in ins[:far]] + list(ins[far:])
    return pl.pallas_call(
        kernel,
        grid=(1,),
        in_specs=[HBM] * far + [whole(a.shape) for a in ins[far:]],
        out_specs=[whole(o.shape) for o in outs],
        out_shape=outs,
        scratch_shapes=scratch,
        compiler_params=pltpu.CompilerParams(vmem_limit_bytes=24 * 1024 * 1024),
        cost_estimate=pl.CostEstimate(flops=flops, bytes_accessed=2_000_000, transcendentals=0),
    )(*ins)


def vmem(shape, dtype=F32):
    return pltpu.VMEM(shape, dtype)


def sems(count):
    return pltpu.SemaphoreType.DMA((count,))


def silu(v):
    return v / (1.0 + jnp.exp(-v))


def pair_lanes(cols, q, rows):
    low = lax.broadcasted_iota(jnp.int32, (rows, LANES), 1) < HEAD_DIM
    first = jnp.broadcast_to(cols[:, 2 * q : 2 * q + 1], (rows, LANES))
    second = jnp.broadcast_to(cols[:, 2 * q + 1 : 2 * q + 2], (rows, LANES))
    return jnp.where(low, first, second)


def fetch(pairs, sems):
    copies = [pltpu.make_async_copy(src, dst, sems.at[k]) for k, (src, dst) in enumerate(pairs)]
    for copy in copies:
        copy.start()
    return copies


def rims_kernel(x_ref, w_ref, r_ref, i_ref, v_ref, out_ref, sems):
    at = 0
    pairs = []
    for ref in (x_ref, w_ref, r_ref, i_ref, v_ref):
        length, width = ref.shape[1:]
        pairs.append((ref.at[0, pl.ds(length - RIM, RIM)], out_ref.at[:, pl.ds(at, width)]))
        at += width
    for copy in fetch(pairs, sems):
        copy.wait()


def filtered(rows, taps, rim, pad_ref):
    length, width = rows.shape
    span = taps.shape[0]
    if rim is None:
        rim = jnp.zeros((RIM, width), F32)
    pad_ref[0:RIM, 0:width] = rim
    pad_ref[RIM : RIM + length, 0:width] = rows
    total = rows * taps[span - 1 : span, :]
    for k in range(span - 1):
        back = span - 1 - k
        total = total + pad_ref[RIM - back : RIM - back + length, 0:width] * taps[k : k + 1, :]
    return total


def column(row):
    size = row.shape[1]
    here = lax.broadcasted_iota(jnp.int32, (size, size), 0) == lax.broadcasted_iota(
        jnp.int32, (size, size), 1
    )
    return jnp.sum(jnp.where(here, jnp.broadcast_to(row, (size, size)), 0.0), axis=1, keepdims=True)


def prepare_kernel(
    x_hbm, w_hbm, xt_hbm, wt_hbm, step_hbm, spike_hbm, off_hbm, rate_hbm,
    xdt_ref, weighted_ref, writes_ref, head_ref, xt_ref, wt_ref, dt_ref, rise_ref, rise_t_ref, remain_ref,
    x_ref, w_ref, step_ref, spike_ref, off_ref, rate_ref, pad_ref, sems,
):
    width = x_hbm.shape[2]
    narrow = w_hbm.shape[2]
    copies = fetch(
        (
            (step_hbm.at[0], step_ref),
            (spike_hbm, spike_ref),
            (off_hbm, off_ref),
            (rate_hbm, rate_ref),
            (w_hbm.at[0], w_ref),
            (wt_hbm, wt_ref),
            (x_hbm.at[0], x_ref),
            (xt_hbm, xt_ref),
            (x_hbm.at[0, pl.ds(0, HEAD)], head_ref.at[:, pl.ds(0, width)]),
            (w_hbm.at[0, pl.ds(0, HEAD)], head_ref.at[:, pl.ds(width, narrow)]),
        ),
        sems,
    )
    for copy in copies[:4]:
        copy.wait()
    heads, length = step_ref.shape
    raw = step_ref[...] + column(off_ref[...])
    dt_t = jnp.maximum(raw, 0.0) + jnp.log1p(jnp.exp(-jnp.abs(raw)))
    fall_t = spike_ref[...] - dt_t * column(jnp.exp(rate_ref[...]))
    row = lax.broadcasted_iota(jnp.int32, (length, length), 0)
    col = lax.broadcasted_iota(jnp.int32, (length, length), 1)
    rise_t = jnp.dot(
        fall_t, (row <= col).astype(F32), precision=lax.Precision.HIGHEST, preferred_element_type=F32
    )
    rise_t_ref[...] = rise_t
    tall = jnp.concatenate([rise_t, dt_t, jnp.zeros((LANES - 2 * heads, length), F32)], axis=0)
    wide = jnp.transpose(tall)
    rise = wide[:, 0:heads]
    dt = wide[:, heads : 2 * heads]
    rise_ref[...] = rise
    dt_ref[...] = dt
    remain = jnp.exp(jnp.minimum(rise[length - 1 : length, :] - rise, 0.0))
    remain_ref[...] = remain
    copies[4].wait()
    copies[5].wait()
    for c in range(0, narrow, STATE):
        cols = slice(c, c + STATE)
        writes_ref[:, cols] = silu(
            filtered(w_ref[:, cols].astype(F32), wt_ref[:, cols].astype(F32), None, pad_ref)
        ).astype(BF16)
    copies[6].wait()
    copies[7].wait()
    for q in range(width // LANES):
        cols = slice(q * LANES, (q + 1) * LANES)
        x = silu(filtered(x_ref[:, cols].astype(F32), xt_ref[:, cols].astype(F32), None, pad_ref))
        x = x * pair_lanes(dt, q, length)
        xdt_ref[:, cols] = x.astype(BF16)
        weighted_ref[:, cols] = (x * pair_lanes(remain, q, length)).astype(BF16)
    copies[8].wait()
    copies[9].wait()


def state_kernel(
    rim_ref, xdt_in, weighted_in, writes_in, head_ref, xt_ref, wt_ref, dt_ref, rise_ref, remain_ref,
    pay_ref, xdt_ref, writes_ref, pad_ref,
):
    length, width = xdt_in.shape
    groups = writes_in.shape[1] // STATE
    per_group = width // LANES // groups
    sub = lax.broadcasted_iota(jnp.int32, (EXTRA, LANES), 0)
    total = rise_ref[length - 1 : length, :]
    dt = dt_ref[0:HEAD, :]
    remain = remain_ref[0:HEAD, :]
    blocks = STATE // 16
    for g in range(groups):
        cols = slice(g * STATE, (g + 1) * STATE)
        spot = slice(width + g * STATE, width + (g + 1) * STATE)
        first = silu(
            filtered(head_ref[:, spot].astype(F32), wt_ref[:, cols].astype(F32), rim_ref[:, spot].astype(F32), pad_ref)
        ).astype(BF16)
        write = jnp.concatenate([first, writes_in[HEAD:, cols]], axis=0)
        writes_ref[:, cols] = write
        write_t = jnp.transpose(write.astype(F32)).astype(BF16)
        for q in range(g * per_group, (g + 1) * per_group):
            cols = slice(q * LANES, (q + 1) * LANES)
            x = silu(
                filtered(head_ref[:, cols].astype(F32), xt_ref[:, cols].astype(F32), rim_ref[:, cols].astype(F32), pad_ref)
            )
            x = x * pair_lanes(dt, q, HEAD)
            xdt_ref[0:HEAD, cols] = x.astype(BF16)
            xdt_ref[HEAD:, cols] = xdt_in[HEAD:, cols]
            x = (x * pair_lanes(remain, q, HEAD)).astype(BF16)
            weighted = jnp.concatenate([x, weighted_in[HEAD:, cols]], axis=0)
            state = jnp.dot(write_t, weighted, preferred_element_type=F32)
            pay_ref[q * blocks : (q + 1) * blocks, 0:16, :] = state.reshape(blocks, 16, LANES).astype(BF16)
            t = pair_lanes(total, q, 1)
            hi = t.astype(BF16).astype(F32)
            mid = (t - hi).astype(BF16).astype(F32)
            lo = t - hi - mid
            terms = jnp.where(sub == 0, hi, jnp.where(sub == 1, mid, jnp.where(sub == 2, lo, 0.0))).astype(BF16)
            pay_ref[q * blocks : (q + 1) * blocks, 16 : 16 + EXTRA, :] = jnp.broadcast_to(terms[None], (blocks, EXTRA, LANES))


def inside_kernel(
    r_hbm, i_hbm, v_hbm, o_hbm, rt_hbm, ct_hbm, gate_hbm, scale_hbm,
    rim_ref, xdt_ref, writes_ref, rise_ref, rise_t_ref,
    inside_ref, reads_ref, conv_ref, open_ref, scale_ref,
    r_ref, i_ref, v_ref, o_ref, rt_ref, ct_ref, gate_ref, pad_ref, sems,
):
    copies = fetch(
        (
            (r_hbm.at[0], r_ref),
            (rt_hbm, rt_ref),
            (i_hbm.at[0], i_ref),
            (v_hbm.at[0], v_ref),
            (o_hbm.at[0], o_ref),
            (ct_hbm, ct_ref),
            (gate_hbm.at[0], gate_ref),
            (scale_hbm, scale_ref),
        ),
        sems,
    )
    length, width = xdt_ref.shape
    groups = writes_ref.shape[1] // STATE
    per_group = width // LANES // groups
    row = lax.broadcasted_iota(jnp.int32, (length, length), 0)
    col = lax.broadcasted_iota(jnp.int32, (length, length), 1)
    causal = row >= col
    rise = rise_ref[...]
    rise_t = rise_t_ref[...]
    low = lax.broadcasted_iota(jnp.int32, (length, LANES), 1) < HEAD_DIM
    base = width + groups * STATE
    copies[0].wait()
    copies[1].wait()
    for g in range(groups):
        cols = slice(g * STATE, (g + 1) * STATE)
        spot = slice(base + g * STATE, base + (g + 1) * STATE)
        read = silu(
            filtered(r_ref[:, cols].astype(F32), rt_ref[:, cols].astype(F32), rim_ref[:, spot].astype(F32), pad_ref)
        ).astype(BF16)
        reads_ref[:, cols] = read
        scores = lax.dot_general(
            read, writes_ref[:, cols], (((1,), (1,)), ((), ())), preferred_element_type=F32
        )
        scores = jnp.where(causal, scores, 0.0)
        for q in range(g * per_group, (g + 1) * per_group):
            both = []
            for h in (2 * q, 2 * q + 1):
                gap = jnp.minimum(rise[:, h : h + 1] - rise_t[h : h + 1, :], 0.0)
                both.append((scores * jnp.exp(gap)).astype(BF16))
            x = xdt_ref[:, q * LANES : (q + 1) * LANES]
            zero = jnp.zeros_like(x)
            stacked = jnp.concatenate([jnp.where(low, x, zero), jnp.where(low, zero, x)], axis=0)
            inside_ref[:, q * LANES : (q + 1) * LANES] = jnp.dot(
                jnp.concatenate(both, axis=1), stacked, preferred_element_type=F32
            )
    for copy in copies[2:]:
        copy.wait()
    for c in range(0, width, LANES):
        open_ref[:, c : c + LANES] = silu(gate_ref[:, c : c + LANES].astype(F32))
    base = base + groups * STATE
    wide = i_ref.shape[1]
    for c in range(0, wide, LANES):
        cols = slice(c, c + LANES)
        product = i_ref[:, cols].astype(F32) * v_ref[:, cols].astype(F32)
        rim = rim_ref[:, base + c : base + c + LANES].astype(F32) * rim_ref[
            :, base + wide + c : base + wide + c + LANES
        ].astype(F32)
        total = filtered(product, ct_ref[:, cols].astype(F32), rim, pad_ref)
        conv_ref[:, cols] = (o_ref[:, cols].astype(F32) * total).astype(BF16)


def scan_kernel(in_ref, out_ref):
    members = in_ref.shape[0]
    carry = jnp.zeros((16, LANES), F32)
    for j in range(members):
        out_ref[j] = carry.astype(BF16)
        if j + 1 < members:
            t = in_ref[j, 16 : 16 + EXTRA, :].astype(F32)
            decay = jnp.exp(t[0:1, :] + t[1:2, :] + t[2:3, :])
            carry = carry * decay + in_ref[j, 0:16, :].astype(F32)


def gate_kernel(p_ref, reads_ref, rise_ref, inside_ref, open_ref, scale_ref, conv_ref, out_ref):
    length, width = inside_ref.shape
    groups = reads_ref.shape[1] // STATE
    per_group = width // LANES // groups
    kept = jnp.exp(rise_ref[...])
    blocks = STATE // 16
    copies = out_ref.shape[0]
    for g in range(groups):
        read = reads_ref[:, g * STATE : (g + 1) * STATE]
        squares = jnp.zeros((length, LANES), F32)
        gated = []
        for q in range(g * per_group, (g + 1) * per_group):
            cols = slice(q * LANES, (q + 1) * LANES)
            before = p_ref[q * blocks : (q + 1) * blocks].reshape(STATE, LANES)
            carried = jnp.dot(read, before, preferred_element_type=F32)
            y = inside_ref[:, cols] + carried * pair_lanes(kept, q, length)
            y = y * open_ref[:, cols]
            squares = squares + y * y
            gated.append(y)
        mean = jnp.sum(squares, axis=1, keepdims=True) * (1.0 / (per_group * LANES))
        inverse = lax.rsqrt(mean + EPS)
        for k, q in enumerate(range(g * per_group, (g + 1) * per_group)):
            cols = slice(q * LANES, (q + 1) * LANES)
            value = (gated[k] * inverse * scale_ref[:, cols]).astype(BF16)
            for c in range(copies):
                out_ref[c, :, cols] = value
    for c in range(copies):
        out_ref[c, :, width:] = conv_ref[...]


def project_kernel(half_ref, a_ref, s_ref, c_ref, out_ref):
    seqs, length, depth = a_ref.shape
    width = s_ref.shape[0]
    start = half_ref[0]
    for k in range(seqs // 2):
        rows = a_ref[start + k]
        out_ref[k] = (
            jnp.dot(rows[:, :width], s_ref[...], preferred_element_type=F32)
            + jnp.dot(rows[:, width:], c_ref[...], preferred_element_type=F32)
        ).astype(out_ref.dtype)


def project(half, rows, s, c, dtype):
    seqs, length, _ = rows.shape
    out = jax.ShapeDtypeStruct((seqs // 2, length, s.shape[1]), dtype)
    ins = (half, rows, s, c)
    return pl.pallas_call(
        project_kernel,
        grid=(1,),
        in_specs=[pl.BlockSpec(memory_space=pltpu.SMEM)] + [whole(a.shape) for a in ins[1:]],
        out_specs=whole(out.shape),
        out_shape=out,
        compiler_params=pltpu.CompilerParams(vmem_limit_bytes=24 * 1024 * 1024),
        cost_estimate=pl.CostEstimate(
            flops=400_000_000, bytes_accessed=2_000_000, transcendentals=0
        ),
    )(*ins)


def merge_kernel(kept_ref, got_ref, out_ref):
    out_ref[...] = (kept_ref[...] + got_ref[...].astype(F32)).astype(BF16)


def per_device(
    output_gate_logits,
    head_input_rows,
    group_state_writes,
    group_state_reads,
    step_logits,
    head_step_offset,
    head_decay_logrates,
    decay_extra_spikes,
    head_input_taps,
    state_input_taps,
    readout_filter_taps,
    grouped_norm_scale,
    convolution_outer_gate,
    convolution_inner_gate,
    convolution_value_rows,
    gated_filter_taps,
    state_output_rows,
    convolution_output_rows,
):
    sds = jax.ShapeDtypeStruct
    _, length, width = head_input_rows.shape
    heads = step_logits.shape[2]
    narrow = group_state_writes.shape[2]
    wide = convolution_inner_gate.shape[2]
    members = lax.axis_size("sp")
    copies = lax.axis_size("fs")
    ends = (
        head_input_rows,
        group_state_writes,
        group_state_reads,
        convolution_inner_gate,
        convolution_value_rows,
    )
    all_width = sum(a.shape[2] for a in ends)
    rims = call(rims_kernel, [sds((RIM, all_width), BF16)], ends, 5, [sems(5)], 1000)[0]
    before = lax.ppermute(rims, "sp", [(k, k + 1) for k in range(members - 1)])
    ins = (
        head_input_rows, group_state_writes, head_input_taps, state_input_taps,
        jnp.swapaxes(step_logits, 1, 2), decay_extra_spikes.T,
        head_step_offset[None], head_decay_logrates[None],
    )
    outs = [
        sds((length, width), BF16),
        sds((length, width), BF16),
        sds((length, narrow), BF16),
        sds((HEAD, width + narrow), BF16),
        sds(head_input_taps.shape, BF16),
        sds(state_input_taps.shape, BF16),
        sds((length, heads), F32),
        sds((length, heads), F32),
        sds((heads, length), F32),
        sds((length, heads), F32),
    ]
    pad = vmem((RIM + length, LANES))
    scratch = [
        vmem((length, width), BF16),
        vmem((length, narrow), BF16),
        vmem((heads, length)),
        vmem((heads, length)),
        vmem((1, heads)),
        vmem((1, heads)),
        pad,
        sems(10),
    ]
    xdt, weighted, writes, head, xt, wt, dt, rise, rise_t, remain = call(
        prepare_kernel, outs, ins, 8, scratch
    )
    ins = (before, xdt, weighted, writes, head, xt, wt, dt, rise, remain)
    outs = [
        sds((members, 16 + EXTRA, LANES), BF16),
        sds((length, width), BF16),
        sds((length, narrow), BF16),
    ]
    payload, xdt, writes = call(state_kernel, outs, ins, 0, [pad])
    gathered = lax.all_to_all(payload, "sp", 0, 0, tiled=True)
    ins = (
        group_state_reads, convolution_inner_gate, convolution_value_rows, convolution_outer_gate,
        readout_filter_taps, gated_filter_taps, output_gate_logits, grouped_norm_scale[None],
        before, xdt, writes, rise, rise_t,
    )
    outs = [
        sds((length, width), F32),
        sds((length, narrow), BF16),
        sds((length, wide), BF16),
        sds((length, width), F32),
        sds((1, width), F32),
    ]
    scratch = [
        vmem((length, narrow), BF16),
        vmem((length, wide), BF16),
        vmem((length, wide), BF16),
        vmem((length, wide), BF16),
        vmem(readout_filter_taps.shape, BF16),
        vmem(gated_filter_taps.shape, BF16),
        vmem((length, width), BF16),
        pad,
        sems(8),
    ]
    inside, reads, conv, opened, scale = call(inside_kernel, outs, ins, 8, scratch)
    prefixes = call(scan_kernel, [sds((members, 16, LANES), BF16)], (gathered,))[0]
    incoming = lax.all_to_all(prefixes, "sp", 0, 0, tiled=True)
    ins = (incoming, reads, rise, inside, opened, scale, conv)
    joined = call(gate_kernel, [sds((copies, length, width + wide), BF16)], ins)[0]
    rows = lax.all_to_all(joined, "fs", 0, 0, tiled=True)
    core = lax.axis_index("tp")
    seqs = copies
    mine = (core * (seqs // 2)).astype(jnp.int32)[None]
    theirs = ((1 - core) * (seqs // 2)).astype(jnp.int32)[None]
    sent = project(theirs, rows, state_output_rows, convolution_output_rows, BF16)
    got = lax.ppermute(sent, "tp", [(0, 1), (1, 0)])
    kept = project(mine, rows, state_output_rows, convolution_output_rows, F32)
    return call(merge_kernel, [sds(got.shape, BF16)], (kept, got))[0]


def solution(mesh):
    return jax.shard_map(
        per_device,
        mesh=mesh,
        in_specs=(
            P("fs", "sp", "tp"),
            P("fs", "sp", "tp"),
            P("fs", "sp", "tp"),
            P("fs", "sp", "tp"),
            P("fs", "sp", "tp"),
            P("tp"),
            P("tp"),
            P("sp", "tp"),
            P(None, "tp"),
            P(None, "tp"),
            P(None, "tp"),
            P("tp"),
            P("fs", "sp", "tp"),
            P("fs", "sp", "tp"),
            P("fs", "sp", "tp"),
            P(None, "tp"),
            P("tp", "fs"),
            P("tp", "fs"),
        ),
        out_specs=P("tp", "sp", "fs"),
        check_vma=False,
    )
```

time: 132 us -> 91.7 us (0.69)
  starting transfers between devices: 41 us -> 21.7 us
  local copies, waits for them, and re-layouts: 16.3 us -> 0.01 us
  Pallas kernels: 0 us -> 10.5 us
  other arithmetic: 6.85 us -> 0 us
  matrix products: 6.58 us -> 0 us
  waiting for transfers between devices: 30.6 us -> 28 us
  blocking collectives: 29.3 us -> 30.8 us
    all_to_all x4 -> x2, starting transfers between devices: 37 us -> 10.8 us  [the longest x1 6.66 us: per_device(): incoming = lax.all_to_all(prefixes, 'sp', 0, 0, tiled=True)]
    pallas_call x0 -> x9, Pallas kernels: none -> 10.5 us  [the longest x7 9.34 us: call(): pl.pallas_call(kernel, grid=(1,), in_specs=[HBM] * far + [whole(a.shape)...]
    ppermute x1 -> x2, starting transfers between devices: 4.01 us -> 10.9 us  [the longest x1 6.89 us: per_device(): got = lax.ppermute(sent, 'tp', [(0, 1), (1, 0)])]
    unnamed x27 -> x4, local copies, waits for them, and re-layouts: 6.79 us -> 0.01 us
    dot_general x8 -> x0, matrix products: 6.58 us -> none  [the longest x1 2.25 us: advance(): jnp.einsum('bgls,blsgr,bsgrp->blgrp', scores, weights, drive, precision=H...]
    slice x7 -> x0, local copies, waits for them, and re-layouts: 3.57 us -> none  [the longest x4 3.34 us: causal_filter(): total = padded[:, 0:length] * kernel[0]]
    all_to_all x4 -> x2, waiting for transfers between devices: 30.6 us -> 27.4 us  [the longest x1 16.7 us: per_device(): rows = lax.all_to_all(joined, 'fs', 0, 0, tiled=True)]
    mul x6 -> x0, other arithmetic: 3.04 us -> none  [the longest x1 1.44 us: per_device(): jax.nn.silu(causal_filter(head_input_rows.astype(jnp.float32), head_input...]
  transfers between devices with their start and end apart: 5 -> 4, of which waited for: 3 -> 3; matrix products, arithmetic and copies ran while one was open for 14% -> 0% of each run, Pallas kernels for 0% -> 5%
where the time goes in v1:
time: 91.7 us; the launch traced here: 91.1 us
  blocking collectives  30.8 us (34%)
  waiting for transfers between devices  28 us (31%)
  starting transfers between devices  21.7 us (24%)
  Pallas kernels  10.5 us (11%)
    all_to_all x1, blocking collectives, per_device(): gathered = lax.all_to_all(payload, 'sp', 0, 0, tiled=True)  30.8 us
    all_to_all x1, waiting for transfers between devices, per_device(): rows = lax.all_to_all(joined, 'fs', 0, 0, tiled=True)  16.7 us
    all_to_all x1, waiting for transfers between devices, per_device(): incoming = lax.all_to_all(prefixes, 'sp', 0, 0, tiled=True)  10.7 us
    pallas_call x7, Pallas kernels, call(): pl.pallas_call(kernel, grid=(1,), in_specs=[HBM] * far + [whole(a.shape)...  9.34 us
    ppermute x1, starting transfers between devices, per_device(): got = lax.ppermute(sent, 'tp', [(0, 1), (1, 0)])  6.89 us
    all_to_all x1, starting transfers between devices, per_device(): incoming = lax.all_to_all(prefixes, 'sp', 0, 0, tiled=True)  6.66 us
    all_to_all x1, starting transfers between devices, per_device(): rows = lax.all_to_all(joined, 'fs', 0, 0, tiled=True)  4.18 us
    ppermute x1, starting transfers between devices, per_device(): before = lax.ppermute(rims, 'sp', [(k, k + 1) for k in range(members - 1)])  4.02 us
  transfers between devices with their start and end apart: 4, of which 3 were waited for; matrix products, arithmetic and copies ran while one was open for 0% of the time, Pallas kernels for 5%

profile of v1, /device:TPU:1, one launch (start us, length us, event | category | flops | bytes accessed | tf_op | source)
XLA Modules:
  0.0 91.1 jit_solution(10796519535432706266)
XLA Ops:
  0.0 0.8 shard_map.172
  0.8 4.0 %collective-permute-start = (bf16[8,2560]{1,0:T(8,128)(2,1)S(1)}, bf16[8,2560]{1,0:T(8,128)(2,1)S(1)}, u32[]{:S(2)}, u32[]{:S(2)}) collective-permute-start(bf16[8,2560]{1,0:T(8,128)(2,1)S(1)} %shard_map.172), channel_id=1, source_target_pairs={{0,8},{8,16},{16,24},{24,32},{32,40},{40,48},{48,56},{56,64},{64,7... | collective-permute-start | bytes 122888 | tf_op jit(solution)/shard_map/ppermute | solution.py:380
  4.8 2.0 %shard_map.173 = (bf16[128,1024]{1,0:T(8,128)(2,1)S(1)}, bf16[128,1024]{1,0:T(8,128)(2,1)S(1)}, bf16[128,256]{1,0:T(8,128)(2,1)S(1)}, bf16[16,1280]{1,0:T(8,128)...) custom-call(bf16[1,128,1024]{2,1,0:T(8,128)(2,1)} %x_hbm.1, ...), custom_call_target="tpu_custom_call" | custom-call | flops 50000000 | bytes 2000000 | tf_op jit(solution)/shard_map/pallas_call | solution.py:28
  6.8 0.0 collective-permute-done.rim_ref
  6.9 0.4 shard_map.174
  7.3 30.8 %all_to_all.15.in_ref = bf16[64,24,128]{2,1,0:T(8,128)(2,1)S(1)} all-to-all(bf16[64,24,128]{2,1,0:T(8,128)(2,1)S(1)} %get-tuple-element.32), channel_id=1, replica_groups=mesh['sp'=64,'fs'=4,'tp'=2] {'sp'}, dimensions={0} | all-to-all | bytes 786432 | tf_op jit(solution)/shard_map/all_to_all | solution.py:419
  38.0 0.8 shard_map.175
  38.9 6.7 %all-to-all-start.1 = ((bf16[64,16,128]{2,1,0:T(8,128)(2,1)}), bf16[64,16,128]{2,1,0:T(8,128)(2,1)S(1)}, u32[]{:S(2)}, u32[]{:S(2)}) async-start(bf16[64,16,128]{2,1,0:T(8,128)(2,1)} %shard_map.175), calls=%async_computation.1 | async-start | bytes 524288 | tf_op jit(solution)/shard_map/all_to_all | solution.py:445
  45.5 1.8 %shard_map.176 = (f32[128,1024]{1,0:T(8,128)S(1)}, bf16[128,256]{1,0:T(8,128)(2,1)S(1)}, bf16[128,512]{1,0:T(8,128)(2,1)S(1)}, f32[128,1024]{1,0:T(8,128)S(1)}, f32[1,1024]{1,0:T(1,128)S(1)}) custom-call(bf16[1,128,256]{2,1,0:T(8,128)(2,1)} %r_hbm.1, bf16[1,128,512]{2,1,0:T(8,128)(2,1)} %i_hbm.1, bf16[1,128,512]{2,1,0:T(8,128)(2,1)} %v_hbm.1, ...), custom_call_target="tpu_custom_call" | custom-call | flops 50000000 | bytes 2000000 | tf_op jit(solution)/shard_map/pallas_call | solution.py:28
  47.4 10.7 %all-to-all-done.1.p_ref = bf16[64,16,128]{2,1,0:T(8,128)(2,1)S(1)} async-done(((bf16[64,16,128]{2,1,0:T(8,128)(2,1)}), bf16[64,16,128]{2,1,0:T(8,128)(2,1)S(1)}, u32[]{:S(2)}, u32[]{:S(2)}) %all-to-all-start.1) | async-done | bytes 262176 | tf_op jit(solution)/shard_map/all_to_all | solution.py:445
  58.0 1.8 %shard_map.177 = bf16[4,128,1536]{2,1,0:T(8,128)(2,1)} custom-call(bf16[64,16,128]{2,1,0:T(8,128)(2,1)S(1)} %all-to-all-done.1.p_ref, bf16[128,256]{1,0:T(8,128)(2,1)S(1)} %get-tuple-element.36.reads_ref, f32[128,16]{1,0:T(8,128)S(1)} %get-tuple-element.30.rise_ref, f32[128,1024]{1,0:T(8,128)S(1)} %get-tuple-element.37.inside_ref, ...), custom_call_target="tpu_custom_call" | custom-call | flops 50000000 | bytes 2000000 | tf_op jit(solution)/shard_map/pallas_call | solution.py:28
  59.8 0.0 copy-start
  59.8 0.0 copy-start.1
  59.8 4.2 %all-to-all-start.2 = ((bf16[4,128,1536]{2,1,0:T(8,128)(2,1)}), bf16[4,128,1536]{2,1,0:T(8,128)(2,1)S(1)}, u32[]{:S(2)}, u32[]{:S(2)}) async-start(bf16[4,128,1536]{2,1,0:T(8,128)(2,1)} %shard_map.177), calls=%async_computation.2 | async-start | bytes 3145728 | tf_op jit(solution)/shard_map/all_to_all | solution.py:448
  64.0 16.7 %all-to-all-done.2.a_ref = bf16[4,128,1536]{2,1,0:T(8,128)(2,1)S(1)} async-done(((bf16[4,128,1536]{2,1,0:T(8,128)(2,1)}), bf16[4,128,1536]{2,1,0:T(8,128)(2,1)S(1)}, u32[]{:S(2)}, u32[]{:S(2)}) %all-to-all-start.2) | async-done | bytes 1572896 | tf_op jit(solution)/shard_map/all_to_all | solution.py:448
  80.7 0.0 copy-done
  80.7 0.0 copy-done.1
  80.7 0.6 shard_map.179
  81.3 6.9 %collective-permute-start.1 = (bf16[2,128,512]{2,1,0:T(8,128)(2,1)S(1)}, bf16[2,128,512]{2,1,0:T(8,128)(2,1)}, u32[]{:S(2)}, u32[]{:S(2)}) collective-permute-start(bf16[2,128,512]{2,1,0:T(8,128)(2,1)S(1)} %shard_map.179), channel_id=1, source_target_pairs={{0,1},{1,0},{2,3},{3,2},{4,5},{5,4},{6,7},{7,6},{8,9},{9,8},{10,11... | collective-permute-start | bytes 786440 | tf_op jit(solution)/shard_map/ppermute | solution.py:454
  88.2 0.6 shard_map.178.kept_ref
  88.8 0.7 collective-permute-done.1.got_ref
  89.4 1.7 %shard_map.180 = bf16[2,128,512]{2,1,0:T(8,128)(2,1)} custom-call(f32[2,128,512]{2,1,0:T(8,128)S(1)} %shard_map.178.kept_ref, bf16[2,128,512]{2,1,0:T(8,128)(2,1)} %collective-permute-done.1.got_ref), custom_call_target="tpu_custom_call" | custom-call | flops 50000000 | bytes 2000000 | tf_op jit(solution)/shard_map/pallas_call | solution.py:28
Async XLA Ops:
  0.8 6.0 %collective-permute-start = (bf16[8,2560]{1,0:T(8,128)(2,1)S(1)}, bf16[8,2560]{1,0:T(8,128)(2,1)S(1)}, u32[]{:S(2)}, u32[]{:S(2)}) collective-permute-start(bf16[8,2560]{1,0:T(8,128)(2,1)S(1)} %shard_map.172), channel_id=1, source_target_pairs={{0,8},{8,16},{16,24},{24,32},{32,40},{40,48},{48,56},{56,64},{64,7... | collective-permute-start | bytes 122888 | tf_op jit(solution)/shard_map/ppermute | solution.py:380
  38.9 19.1 %all-to-all-start.1 = ((bf16[64,16,128]{2,1,0:T(8,128)(2,1)}), bf16[64,16,128]{2,1,0:T(8,128)(2,1)S(1)}, u32[]{:S(2)}, u32[]{:S(2)}) async-start(bf16[64,16,128]{2,1,0:T(8,128)(2,1)} %shard_map.175), calls=%async_computation.1 | async-start | bytes 524288 | tf_op jit(solution)/shard_map/all_to_all | solution.py:445
  59.8 20.9 %copy-start = (bf16[1024,512]{1,0:T(8,128)(2,1)S(1)}, bf16[1024,512]{1,0:T(8,128)(2,1)}, u32[]{:S(2)}) copy-start(bf16[1024,512]{1,0:T(8,128)(2,1)} %s_ref.3) | copy-start | bytes 3145732
  59.8 20.9 %copy-start.1 = (bf16[512,512]{1,0:T(8,128)(2,1)S(1)}, bf16[512,512]{1,0:T(8,128)(2,1)}, u32[]{:S(2)}) copy-start(bf16[512,512]{1,0:T(8,128)(2,1)} %c_ref.3) | copy-start | bytes 1572868
  59.8 20.9 %all-to-all-start.2 = ((bf16[4,128,1536]{2,1,0:T(8,128)(2,1)}), bf16[4,128,1536]{2,1,0:T(8,128)(2,1)S(1)}, u32[]{:S(2)}, u32[]{:S(2)}) async-start(bf16[4,128,1536]{2,1,0:T(8,128)(2,1)} %shard_map.177), calls=%async_computation.2 | async-start | bytes 3145728 | tf_op jit(solution)/shard_map/all_to_all | solution.py:448
  81.3 8.2 %collective-permute-start.1 = (bf16[2,128,512]{2,1,0:T(8,128)(2,1)S(1)}, bf16[2,128,512]{2,1,0:T(8,128)(2,1)}, u32[]{:S(2)}, u32[]{:S(2)}) collective-permute-start(bf16[2,128,512]{2,1,0:T(8,128)(2,1)S(1)} %shard_map.179), channel_id=1, source_target_pairs={{0,1},{1,0},{2,3},{3,2},{4,5},{5,4},{6,7},{7,6},{8,9},{9,8},{10,11... | collective-permute-start | bytes 786440 | tf_op jit(solution)/shard_map/ppermute | solution.py:454

commit v2 on v1

v2 whole, which is shorter than its diff:
```python
import jax
import jax.numpy as jnp
from jax import lax
from jax.experimental import pallas as pl
from jax.experimental.pallas import tpu as pltpu
from jax.sharding import PartitionSpec as P

EPS = 1e-06
F32 = jnp.float32
BF16 = jnp.bfloat16
STATE = 128
LANES = 128
HEAD_DIM = 64
EXTRA = 8
PAD = 8
RIM = 4
HEAD = 16
FIRST_OUT = 52
FIRST_BACK = 52


def whole(shape):
    return pl.BlockSpec(shape, lambda *_: (0,) * len(shape))


HBM = pl.BlockSpec(memory_space=pltpu.HBM)


def call(kernel, outs, ins, far=0, scratch=(), flops=50_000_000):
    ins = [pltpu.with_memory_space_constraint(a, pltpu.HBM) for a in ins[:far]] + list(ins[far:])
    return pl.pallas_call(
        kernel,
        grid=(1,),
        in_specs=[HBM] * far + [whole(a.shape) for a in ins[far:]],
        out_specs=[whole(o.shape) for o in outs],
        out_shape=outs,
        scratch_shapes=scratch,
        compiler_params=pltpu.CompilerParams(vmem_limit_bytes=24 * 1024 * 1024),
        cost_estimate=pl.CostEstimate(flops=flops, bytes_accessed=2_000_000, transcendentals=0),
    )(*ins)


def vmem(shape, dtype=F32):
    return pltpu.VMEM(shape, dtype)


def sems(count):
    return pltpu.SemaphoreType.DMA((count,))


def silu(v):
    return v / (1.0 + jnp.exp(-v))


def pair_lanes(cols, q, rows):
    low = lax.broadcasted_iota(jnp.int32, (rows, LANES), 1) < HEAD_DIM
    first = jnp.broadcast_to(cols[:, 2 * q : 2 * q + 1], (rows, LANES))
    second = jnp.broadcast_to(cols[:, 2 * q + 1 : 2 * q + 2], (rows, LANES))
    return jnp.where(low, first, second)


def fetch(pairs, sems):
    copies = [pltpu.make_async_copy(src, dst, sems.at[k]) for k, (src, dst) in enumerate(pairs)]
    for copy in copies:
        copy.start()
    return copies


def rims_kernel(x_ref, w_ref, r_ref, i_ref, v_ref, out_ref, rows_ref, sems):
    at = 0
    pairs = []
    for ref in (x_ref, w_ref, r_ref, i_ref, v_ref):
        length, width = ref.shape[1:]
        pairs.append((ref.at[0, pl.ds(length - PAD, PAD)], rows_ref.at[:, pl.ds(at, width)]))
        at += width
    for copy in fetch(pairs, sems):
        copy.wait()
    out_ref[...] = rows_ref[PAD - RIM :, :]


def filtered(rows, taps, rim, pad_ref):
    length, width = rows.shape
    span = taps.shape[0]
    if rim is None:
        rim = jnp.zeros((RIM, width), F32)
    pad_ref[PAD - RIM : PAD, 0:width] = rim
    pad_ref[PAD : PAD + length, 0:width] = rows
    total = rows * taps[span - 1 : span, :]
    for k in range(span - 1):
        back = span - 1 - k
        total = total + pad_ref[PAD - back : PAD - back + length, 0:width] * taps[k : k + 1, :]
    return total


def column(row):
    size = row.shape[1]
    here = lax.broadcasted_iota(jnp.int32, (size, size), 0) == lax.broadcasted_iota(
        jnp.int32, (size, size), 1
    )
    return jnp.sum(jnp.where(here, jnp.broadcast_to(row, (size, size)), 0.0), axis=1, keepdims=True)


def prepare_kernel(
    x_hbm, w_hbm, r_hbm, i_hbm, v_hbm, o_hbm, gate_hbm, xt_hbm, wt_hbm, rt_hbm, ct_hbm, scale_hbm,
    step_hbm, spike_hbm, off_hbm, rate_hbm,
    weighted_ref, writes_ref, reads_ref, inside_ref, conv_ref, open_ref, head_ref,
    xt_ref, wt_ref, rt_ref, ct_ref, scale_ref, dt_ref, rise_ref, remain_ref,
    x_ref, w_ref, r_ref, i_ref, v_ref, o_ref, gate_ref,
    step_ref, spike_ref, off_ref, rate_ref, pad_ref, sems,
):
    width = x_hbm.shape[2]
    narrow = w_hbm.shape[2]
    broad = i_hbm.shape[2]
    copies = fetch(
        (
            (step_hbm.at[0], step_ref),
            (spike_hbm, spike_ref),
            (off_hbm, off_ref),
            (rate_hbm, rate_ref),
            (w_hbm.at[0], w_ref),
            (wt_hbm, wt_ref),
            (r_hbm.at[0], r_ref),
            (rt_hbm, rt_ref),
            (x_hbm.at[0], x_ref),
            (xt_hbm, xt_ref),
            (gate_hbm.at[0], gate_ref),
            (i_hbm.at[0], i_ref),
            (v_hbm.at[0], v_ref),
            (o_hbm.at[0], o_ref),
            (ct_hbm, ct_ref),
            (scale_hbm, scale_ref),
        ),
        sems,
    )
    for copy in copies[:4]:
        copy.wait()
    heads, length = step_ref.shape
    raw = step_ref[...] + column(off_ref[...])
    dt_t = jnp.maximum(raw, 0.0) + jnp.log1p(jnp.exp(-jnp.abs(raw)))
    fall_t = spike_ref[...] - dt_t * column(jnp.exp(rate_ref[...]))
    row = lax.broadcasted_iota(jnp.int32, (length, length), 0)
    col = lax.broadcasted_iota(jnp.int32, (length, length), 1)
    rise_t = jnp.dot(
        fall_t, (row <= col).astype(F32), precision=lax.Precision.HIGHEST, preferred_element_type=F32
    )
    tall = jnp.concatenate([rise_t, dt_t, jnp.zeros((LANES - 2 * heads, length), F32)], axis=0)
    turned_over = jnp.transpose(tall)
    rise = turned_over[:, 0:heads]
    dt = turned_over[:, heads : 2 * heads]
    rise_ref[...] = rise
    dt_ref[...] = dt[0:HEAD, :]
    remain = jnp.exp(jnp.minimum(rise[length - 1 : length, :] - rise, 0.0))
    remain_ref[...] = remain[0:HEAD, :]
    for copy in copies[4:8]:
        copy.wait()
    groups = narrow // STATE
    per_group = width // LANES // groups
    scores = []
    for g in range(groups):
        cols = slice(g * STATE, (g + 1) * STATE)
        write = silu(
            filtered(w_ref[:, cols].astype(F32), wt_ref[:, cols].astype(F32), None, pad_ref)
        ).astype(BF16)
        read = silu(
            filtered(r_ref[:, cols].astype(F32), rt_ref[:, cols].astype(F32), None, pad_ref)
        ).astype(BF16)
        writes_ref[:, cols] = write
        reads_ref[:, cols] = read
        score = lax.dot_general(read, write, (((1,), (1,)), ((), ())), preferred_element_type=F32)
        scores.append(jnp.where(row >= col, score, 0.0))
    for copy in copies[8:10]:
        copy.wait()
    low = lax.broadcasted_iota(jnp.int32, (length, LANES), 1) < HEAD_DIM
    late = lax.broadcasted_iota(jnp.int32, (length, LANES), 0) >= HEAD
    for q in range(width // LANES):
        cols = slice(q * LANES, (q + 1) * LANES)
        x = silu(filtered(x_ref[:, cols].astype(F32), xt_ref[:, cols].astype(F32), None, pad_ref))
        x = x * pair_lanes(dt, q, length)
        weighted_ref[:, cols] = (x * pair_lanes(remain, q, length)).astype(BF16)
        stacked = jnp.concatenate(
            [
                jnp.where(low & late, x, 0.0).astype(BF16),
                jnp.where(late & ~low, x, 0.0).astype(BF16),
            ],
            axis=0,
        )
        both = []
        for h in (2 * q, 2 * q + 1):
            gap = jnp.minimum(rise[:, h : h + 1] - rise_t[h : h + 1, :], 0.0)
            both.append((scores[q // per_group] * jnp.exp(gap)).astype(BF16))
        inside_ref[:, cols] = jnp.dot(
            jnp.concatenate(both, axis=1), stacked, preferred_element_type=F32
        )
    for copy in copies[10:]:
        copy.wait()
    for c in range(0, width, LANES):
        open_ref[:, c : c + LANES] = silu(gate_ref[:, c : c + LANES].astype(F32))
    for c in range(0, broad, LANES):
        cols = slice(c, c + LANES)
        product = i_ref[:, cols].astype(F32) * v_ref[:, cols].astype(F32)
        total = filtered(product, ct_ref[:, cols].astype(F32), None, pad_ref)
        conv_ref[:, cols] = (o_ref[:, cols].astype(F32) * total).astype(BF16)
    at = 0
    for ref in (x_ref, w_ref, r_ref, i_ref, v_ref, o_ref):
        head_ref[:, at : at + ref.shape[1]] = ref[0:HEAD, :]
        at += ref.shape[1]


def state_kernel(
    rim_ref, weighted_ref, writes_ref, reads_in, inside_in, conv_in, head_ref,
    xt_ref, wt_ref, rt_ref, ct_ref, dt_ref, rise_ref, remain_ref,
    pay_ref, reads_ref, inside_ref, conv_ref, pad_ref,
):
    length, width = weighted_ref.shape
    heads = rise_ref.shape[1]
    narrow = writes_ref.shape[1]
    broad = conv_in.shape[1]
    groups = narrow // STATE
    per_group = width // LANES // groups
    sub = lax.broadcasted_iota(jnp.int32, (EXTRA, LANES), 0)
    rise = rise_ref[...]
    total = rise[length - 1 : length, :]
    dt = dt_ref[...]
    remain = remain_ref[...]
    blocks = STATE // 16

    def first(taps_ref, cols, spot):
        return silu(
            filtered(
                head_ref[:, spot].astype(F32),
                taps_ref[:, cols].astype(F32),
                rim_ref[:, spot].astype(F32),
                pad_ref,
            )
        )

    lane = lax.broadcasted_iota(jnp.int32, (length, LANES), 1)
    row = lax.broadcasted_iota(jnp.int32, (length, LANES), 0)
    share = heads // groups
    for g in range(groups):
        cols = slice(g * STATE, (g + 1) * STATE)
        spot = slice(width + g * STATE, width + (g + 1) * STATE)
        first_write = first(wt_ref, cols, spot).astype(BF16)
        write = jnp.concatenate([first_write, writes_ref[HEAD:, cols]], axis=0)
        write_t = jnp.transpose(write.astype(F32)).astype(BF16)
        firsts = []
        for q in range(g * per_group, (g + 1) * per_group):
            pair = slice(q * LANES, (q + 1) * LANES)
            x = first(xt_ref, pair, pair) * pair_lanes(dt, q, HEAD)
            firsts.append(x.astype(BF16))
            x = (x * pair_lanes(remain, q, HEAD)).astype(BF16)
            weighted = jnp.concatenate([x, weighted_ref[HEAD:, pair]], axis=0)
            state = jnp.dot(write_t, weighted, preferred_element_type=F32)
            pay_ref[q * blocks : (q + 1) * blocks, 0:16, :] = state.reshape(blocks, 16, LANES).astype(BF16)
            t = pair_lanes(total, q, 1)
            hi = t.astype(BF16).astype(F32)
            mid = (t - hi).astype(BF16).astype(F32)
            lo = t - hi - mid
            terms = jnp.where(sub == 0, hi, jnp.where(sub == 1, mid, jnp.where(sub == 2, lo, 0.0))).astype(BF16)
            pay_ref[q * blocks : (q + 1) * blocks, 16 : 16 + EXTRA, :] = jnp.broadcast_to(terms[None], (blocks, EXTRA, LANES))
        spot = slice(width + narrow + g * STATE, width + narrow + (g + 1) * STATE)
        read = jnp.concatenate([first(rt_ref, cols, spot).astype(BF16), reads_in[HEAD:, cols]], axis=0)
        reads_ref[:, cols] = read
        scores = lax.dot_general(
            read, jnp.concatenate([first_write] * share, axis=0), (((1,), (1,)), ((), ())),
            preferred_element_type=F32,
        )
        spread = (
            lax.broadcasted_iota(jnp.int32, (heads, LANES), 0)
            == g * share + lax.broadcasted_iota(jnp.int32, (heads, LANES), 1) // HEAD
        ).astype(F32)
        rises = jnp.dot(rise, spread, precision=lax.Precision.HIGHEST, preferred_element_type=F32)
        here = (row == lane % HEAD)[0:HEAD]
        start = jnp.sum(jnp.where(here, rises[0:HEAD], 0.0), axis=0, keepdims=True)
        kept = jnp.where(
            lane % HEAD <= row, scores * jnp.exp(jnp.minimum(rises - start, 0.0)), 0.0
        ).astype(BF16)
        span = per_group * LANES
        tiled = jnp.concatenate([jnp.concatenate(firsts, axis=1)] * share, axis=0)
        own = (
            lax.broadcasted_iota(jnp.int32, (LANES, span), 0) // HEAD
            == lax.broadcasted_iota(jnp.int32, (LANES, span), 1) // HEAD_DIM
        )
        tiled = jnp.where(own, tiled, jnp.zeros_like(tiled))
        wide = slice(g * span, (g + 1) * span)
        inside_ref[:, wide] = inside_in[:, wide] + jnp.dot(kept, tiled, preferred_element_type=F32)
    base = width + 2 * narrow
    for c in range(0, broad, LANES):
        cols = slice(c, c + LANES)
        i = slice(base + c, base + c + LANES)
        v = slice(base + broad + c, base + broad + c + LANES)
        o = slice(base + 2 * broad + c, base + 2 * broad + c + LANES)
        product = head_ref[:, i].astype(F32) * head_ref[:, v].astype(F32)
        rim = rim_ref[:, i].astype(F32) * rim_ref[:, v].astype(F32)
        value = filtered(product, ct_ref[:, cols].astype(F32), rim, pad_ref)
        conv_ref[0:HEAD, cols] = (head_ref[:, o].astype(F32) * value).astype(BF16)
        conv_ref[HEAD:, cols] = conv_in[HEAD:, cols]


def turned(members, first):
    return [[(k + first) % members for k in range(members)]]


def scan_kernel(in_ref, out_ref):
    members = in_ref.shape[0]
    carry = jnp.zeros((16, LANES), F32)
    for j in range(members):
        at = (j - FIRST_OUT) % members
        out_ref[(j - FIRST_BACK) % members] = carry.astype(BF16)
        if j + 1 < members:
            t = in_ref[at, 16 : 16 + EXTRA, :].astype(F32)
            decay = jnp.exp(t[0:1, :] + t[1:2, :] + t[2:3, :])
            carry = carry * decay + in_ref[at, 0:16, :].astype(F32)


def gate_kernel(p_ref, reads_ref, rise_ref, inside_ref, open_ref, scale_ref, conv_ref, out_ref):
    length, width = inside_ref.shape
    groups = reads_ref.shape[1] // STATE
    per_group = width // LANES // groups
    kept = jnp.exp(rise_ref[...])
    blocks = STATE // 16
    copies = out_ref.shape[0]
    for g in range(groups):
        read = reads_ref[:, g * STATE : (g + 1) * STATE]
        squares = jnp.zeros((length, LANES), F32)
        gated = []
        for q in range(g * per_group, (g + 1) * per_group):
            cols = slice(q * LANES, (q + 1) * LANES)
            spots = [(q * blocks + k + FIRST_OUT - FIRST_BACK) % p_ref.shape[0] for k in range(blocks)]
            before = jnp.concatenate([p_ref[spot] for spot in spots], axis=0)
            carried = jnp.dot(read, before, preferred_element_type=F32)
            y = inside_ref[:, cols] + carried * pair_lanes(kept, q, length)
            y = y * open_ref[:, cols]
            squares = squares + y * y
            gated.append(y)
        mean = jnp.sum(squares, axis=1, keepdims=True) * (1.0 / (per_group * LANES))
        inverse = lax.rsqrt(mean + EPS)
        for k, q in enumerate(range(g * per_group, (g + 1) * per_group)):
            cols = slice(q * LANES, (q + 1) * LANES)
            value = (gated[k] * inverse * scale_ref[:, cols]).astype(BF16)
            for c in range(copies):
                out_ref[c, :, cols] = value
    for c in range(copies):
        out_ref[c, :, width:] = conv_ref[...]


def project_kernel(half_ref, a_ref, s_ref, c_ref, out_ref):
    seqs, length, depth = a_ref.shape
    width = s_ref.shape[0]
    start = half_ref[0]
    for k in range(seqs // 2):
        rows = a_ref[start + k]
        out_ref[k] = (
            jnp.dot(rows[:, :width], s_ref[...], preferred_element_type=F32)
            + jnp.dot(rows[:, width:], c_ref[...], preferred_element_type=F32)
        ).astype(out_ref.dtype)


def project(half, rows, s, c, dtype):
    seqs, length, _ = rows.shape
    out = jax.ShapeDtypeStruct((seqs // 2, length, s.shape[1]), dtype)
    ins = (half, rows, s, c)
    return pl.pallas_call(
        project_kernel,
        grid=(1,),
        in_specs=[pl.BlockSpec(memory_space=pltpu.SMEM)] + [whole(a.shape) for a in ins[1:]],
        out_specs=whole(out.shape),
        out_shape=out,
        compiler_params=pltpu.CompilerParams(vmem_limit_bytes=24 * 1024 * 1024),
        cost_estimate=pl.CostEstimate(
            flops=400_000_000, bytes_accessed=2_000_000, transcendentals=0
        ),
    )(*ins)


def merge_kernel(kept_ref, got_ref, out_ref):
    out_ref[...] = (kept_ref[...] + got_ref[...].astype(F32)).astype(BF16)


def per_device(
    output_gate_logits,
    head_input_rows,
    group_state_writes,
    group_state_reads,
    step_logits,
    head_step_offset,
    head_decay_logrates,
    decay_extra_spikes,
    head_input_taps,
    state_input_taps,
    readout_filter_taps,
    grouped_norm_scale,
    convolution_outer_gate,
    convolution_inner_gate,
    convolution_value_rows,
    gated_filter_taps,
    state_output_rows,
    convolution_output_rows,
):
    sds = jax.ShapeDtypeStruct
    _, length, width = head_input_rows.shape
    heads = step_logits.shape[2]
    narrow = group_state_writes.shape[2]
    wide = convolution_inner_gate.shape[2]
    members = lax.axis_size("sp")
    copies = lax.axis_size("fs")
    ends = (
        head_input_rows,
        group_state_writes,
        group_state_reads,
        convolution_inner_gate,
        convolution_value_rows,
    )
    all_width = sum(a.shape[2] for a in ends)
    rims = call(
        rims_kernel, [sds((RIM, all_width), BF16)], ends, 5, [vmem((PAD, all_width), BF16), sems(5)], 1000
    )[0]
    before = lax.ppermute(rims, "sp", [(k, k + 1) for k in range(members - 1)])
    ins = (
        *ends, convolution_outer_gate, output_gate_logits,
        head_input_taps, state_input_taps, readout_filter_taps, gated_filter_taps,
        grouped_norm_scale[None], jnp.swapaxes(step_logits, 1, 2), decay_extra_spikes.T,
        head_step_offset[None], head_decay_logrates[None],
    )
    tall = sds((length, width), BF16)
    slim = sds((length, narrow), BF16)
    side = sds((length, wide), BF16)
    full = sds((length, width), F32)
    outs = [
        tall, slim, slim, full, side, full, sds((HEAD, all_width + wide), BF16),
        sds(head_input_taps.shape, BF16), sds(state_input_taps.shape, BF16),
        sds(readout_filter_taps.shape, BF16), sds(gated_filter_taps.shape, BF16),
        sds((1, width), F32), sds((HEAD, heads), F32), sds((length, heads), F32), sds((HEAD, heads), F32),
    ]
    pad = vmem((PAD + length, LANES))
    scratch = [vmem(a.shape[1:], BF16) for a in ins[:7]] + [
        vmem((heads, length)),
        vmem((heads, length)),
        vmem((1, heads)),
        vmem((1, heads)),
        pad,
        sems(16),
    ]
    (
        weighted, writes, reads, inside, conv, opened, head, xt, wt, rt, ct, scale, dt, rise, remain,
    ) = call(prepare_kernel, outs, ins, 16, scratch)
    ins = (before, weighted, writes, reads, inside, conv, head, xt, wt, rt, ct, dt, rise, remain)
    outs = [sds((members, 16 + EXTRA, LANES), BF16), slim, full, side]
    payload, reads, inside, conv = call(state_kernel, outs, ins, 0, [pad])
    core = lax.axis_index("tp")
    seqs = copies
    mine = (core * (seqs // 2)).astype(jnp.int32)[None]
    theirs = ((1 - core) * (seqs // 2)).astype(jnp.int32)[None]
    payload, mine, theirs = lax.optimization_barrier((payload, mine, theirs))
    gathered = lax.all_to_all(
        payload, "sp", 0, 0, axis_index_groups=turned(members, FIRST_OUT), tiled=True
    )
    prefixes = call(scan_kernel, [sds((members, 16, LANES), BF16)], (gathered,))[0]
    incoming = lax.all_to_all(prefixes, "sp", 0, 0, axis_index_groups=turned(members, FIRST_BACK), tiled=True)
    ins = (incoming, reads, rise, inside, opened, scale, conv)
    joined = call(gate_kernel, [sds((copies, length, width + wide), BF16)], ins)[0]
    rows = lax.all_to_all(joined, "fs", 0, 0, tiled=True)
    sent = project(theirs, rows, state_output_rows, convolution_output_rows, BF16)
    got = lax.ppermute(sent, "tp", [(0, 1), (1, 0)])
    kept = project(mine, rows, state_output_rows, convolution_output_rows, F32)
    return call(merge_kernel, [sds(got.shape, BF16)], (kept, got))[0]


def solution(mesh):
    return jax.shard_map(
        per_device,
        mesh=mesh,
        in_specs=(
            P("fs", "sp", "tp"),
            P("fs", "sp", "tp"),
            P("fs", "sp", "tp"),
            P("fs", "sp", "tp"),
            P("fs", "sp", "tp"),
            P("tp"),
            P("tp"),
            P("sp", "tp"),
            P(None, "tp"),
            P(None, "tp"),
            P(None, "tp"),
            P("tp"),
            P("fs", "sp", "tp"),
            P("fs", "sp", "tp"),
            P("fs", "sp", "tp"),
            P(None, "tp"),
            P("tp", "fs"),
            P("tp", "fs"),
        ),
        out_specs=P("tp", "sp", "fs"),
        check_vma=False,
    )
```

time: 91.7 us -> 86.5 us (0.943)
  blocking collectives: 30.8 us -> 68.7 us
  waiting for transfers between devices: 28 us -> 0.55 us
  starting transfers between devices: 21.7 us -> 9.29 us
  Pallas kernels: 10.5 us -> 7.4 us
    all_to_all x1 -> x3, blocking collectives: 30.8 us -> 68.7 us  [the longest x1 28 us: per_device(): lax.all_to_all(payload, 'sp', 0, 0, axis_index_groups=turned(members, FIR...]
    all_to_all x2 -> x0, waiting for transfers between devices: 27.4 us -> none  [the longest x1 16.7 us: per_device(): rows = lax.all_to_all(joined, 'fs', 0, 0, tiled=True)]
    all_to_all x2 -> x0, starting transfers between devices: 10.8 us -> none  [the longest x1 6.66 us: per_device(): incoming = lax.all_to_all(prefixes, 'sp', 0, 0, tiled=True)]
    pallas_call x7 -> x6, Pallas kernels: 9.34 us -> 6.25 us  [call(): pl.pallas_call(kernel, grid=(1,), in_specs=[HBM] * far + [whole(a.shape)...]
    ppermute x1, starting transfers between devices: 6.89 us -> 5.27 us  [per_device(): got = lax.ppermute(sent, 'tp', [(0, 1), (1, 0)])]
  transfers between devices with their start and end apart: 4 -> 2, of which waited for: 3 -> 1; matrix products, arithmetic and copies ran while one was open for 0% -> 0% of each run, Pallas kernels for 5% -> 4%
where the time goes in v2:
time: 86.5 us; the launch traced here: 86 us
  blocking collectives  68.7 us (79%)
  starting transfers between devices  9.29 us (11%)
  Pallas kernels  7.4 us (9%)
    all_to_all x1, blocking collectives, per_device(): lax.all_to_all(payload, 'sp', 0, 0, axis_index_groups=turned(members, FIR...  28 us
    all_to_all x1, blocking collectives, per_device(): rows = lax.all_to_all(joined, 'fs', 0, 0, tiled=True)  22.1 us
    all_to_all x1, blocking collectives, per_device(): lax.all_to_all(prefixes, 'sp', 0, 0, axis_index_groups=turned(members, FI...  18.6 us
    pallas_call x6, Pallas kernels, call(): pl.pallas_call(kernel, grid=(1,), in_specs=[HBM] * far + [whole(a.shape)...  6.25 us
    ppermute x1, starting transfers between devices, per_device(): got = lax.ppermute(sent, 'tp', [(0, 1), (1, 0)])  5.27 us
    ppermute x1, starting transfers between devices, per_device(): before = lax.ppermute(rims, 'sp', [(k, k + 1) for k in range(members - 1)])  4.02 us
  transfers between devices with their start and end apart: 2, of which 1 were waited for; matrix products, arithmetic and copies ran while one was open for 0% of the time, Pallas kernels for 4%

profile of v2, /device:TPU:1, one launch (start us, length us, event | category | flops | bytes accessed | tf_op | source)
XLA Modules:
  0.0 86.0 jit_solution(6928614089446591131)
XLA Ops:
  0.0 0.8 shard_map.172
  0.8 4.0 %collective-permute-start = (bf16[4,2560]{1,0:T(4,128)(2,1)S(1)}, bf16[4,2560]{1,0:T(4,128)(2,1)S(1)}, u32[]{:S(2)}, u32[]{:S(2)}) collective-permute-start(bf16[4,2560]{1,0:T(4,128)(2,1)S(1)} %shard_map.172), channel_id=1, source_target_pairs={{0,8},{8,16},{16,24},{24,32},{32,40},{40,48},{48,56},{56,64},{64,7... | collective-permute-start | bytes 61448 | tf_op jit(solution)/shard_map/ppermute | solution.py:418
  4.9 3.0 %shard_map.173 = (bf16[128,1024]{1,0:T(8,128)(2,1)S(1)}, bf16[128,256]{1,0:T(8,128)(2,1)S(1)}, bf16[128,256]{1,0:T(8,128)(2,1)S(1)}, f32[128,1024]{1,0:T(8,128)S...) custom-call(bf16[1,128,1024]{2,1,0:T(8,128)(2,1)} %x_hbm.1, ...), custom_call_target="tpu_custom_call" | custom-call | flops 50000000 | bytes 2000000 | tf_op jit(solution)/shard_map/pallas_call | solution.py:31
  7.9 0.0 collective-permute-done.rim_ref
  7.9 0.9 shard_map.174
  8.8 28.0 %all_to_all.15.in_ref = bf16[64,24,128]{2,1,0:T(8,128)(2,1)S(1)} all-to-all(bf16[64,24,128]{2,1,0:T(8,128)(2,1)S(1)} %get-tuple-element.42), channel_id=1, replica_groups={{416,424,432,440,448,456,464,472,480,488,496,504,0,8,16,24,32,40,48,56,..., dimensions={0} | all-to-all | bytes 786432 | tf_op jit(solution)/shard_map/all_to_all | solution.py:455
  36.8 0.1 shard_map.175
  37.0 18.6 %all_to_all.16.p_ref = bf16[64,16,128]{2,1,0:T(8,128)(2,1)S(1)} all-to-all(bf16[64,16,128]{2,1,0:T(8,128)(2,1)S(1)} %shard_map.175), channel_id=1, replica_groups={{416,424,432,440,448,456,464,472,480,488,496,504,0,8,16,24,32,40,48,56,..., dimensions={0} | all-to-all | bytes 524288 | tf_op jit(solution)/shard_map/all_to_all | solution.py:459
  55.5 0.7 shard_map.176
  56.2 0.0 copy-start
  56.2 0.0 copy-start.1
  56.2 22.1 %all_to_all.17.a_ref = bf16[4,128,1536]{2,1,0:T(8,128)(2,1)S(1)} all-to-all(bf16[4,128,1536]{2,1,0:T(8,128)(2,1)S(1)} %shard_map.176), channel_id=1, replica_groups=mesh['sp'=64,'fs'=4,'tp'=2] {'fs'}, dimensions={0} | all-to-all | bytes 3145728 | tf_op jit(solution)/shard_map/all_to_all | solution.py:462
  78.3 0.0 copy-done
  78.3 0.0 copy-done.1
  78.3 0.6 shard_map.178
  78.9 5.3 %collective-permute-start.1 = (bf16[2,128,512]{2,1,0:T(8,128)(2,1)S(1)}, bf16[2,128,512]{2,1,0:T(8,128)(2,1)S(1)}, u32[]{:S(2)}, u32[]{:S(2)}) collective-permute-start(bf16[2,128,512]{2,1,0:T(8,128)(2,1)S(1)} %shard_map.178), channel_id=1, source_target_pairs={{0,1},{1,0},{2,3},{3,2},{4,5},{5,4},{6,7},{7,6},{8,9},{9,8},{10,11... | collective-permute-start | bytes 786440 | tf_op jit(solution)/shard_map/ppermute | solution.py:464
  84.1 0.6 shard_map.177.kept_ref
  84.7 0.6 collective-permute-done.1.got_ref
  85.3 0.7 shard_map.179
Async XLA Ops:
  0.8 7.1 %collective-permute-start = (bf16[4,2560]{1,0:T(4,128)(2,1)S(1)}, bf16[4,2560]{1,0:T(4,128)(2,1)S(1)}, u32[]{:S(2)}, u32[]{:S(2)}) collective-permute-start(bf16[4,2560]{1,0:T(4,128)(2,1)S(1)} %shard_map.172), channel_id=1, source_target_pairs={{0,8},{8,16},{16,24},{24,32},{32,40},{40,48},{48,56},{56,64},{64,7... | collective-permute-start | bytes 61448 | tf_op jit(solution)/shard_map/ppermute | solution.py:418
  56.2 22.1 %copy-start = (bf16[1024,512]{1,0:T(8,128)(2,1)S(1)}, bf16[1024,512]{1,0:T(8,128)(2,1)}, u32[]{:S(2)}) copy-start(bf16[1024,512]{1,0:T(8,128)(2,1)} %s_ref.3) | copy-start | bytes 3145732
  56.2 22.1 %copy-start.1 = (bf16[512,512]{1,0:T(8,128)(2,1)S(1)}, bf16[512,512]{1,0:T(8,128)(2,1)}, u32[]{:S(2)}) copy-start(bf16[512,512]{1,0:T(8,128)(2,1)} %c_ref.3) | copy-start | bytes 1572868
  78.9 6.4 %collective-permute-start.1 = (bf16[2,128,512]{2,1,0:T(8,128)(2,1)S(1)}, bf16[2,128,512]{2,1,0:T(8,128)(2,1)S(1)}, u32[]{:S(2)}, u32[]{:S(2)}) collective-permute-start(bf16[2,128,512]{2,1,0:T(8,128)(2,1)S(1)} %shard_map.178), channel_id=1, source_target_pairs={{0,1},{1,0},{2,3},{3,2},{4,5},{5,4},{6,7},{7,6},{8,9},{9,8},{10,11... | collective-permute-start | bytes 786440 | tf_op jit(solution)/shard_map/ppermute | solution.py:464

commit v3 on v2

--- a/solution.py
+++ b/solution.py
@@ -1,9 +1,12 @@
+import functools
+
 import jax
 import jax.numpy as jnp
 from jax import lax
 from jax.experimental import pallas as pl
 from jax.experimental.pallas import tpu as pltpu
 from jax.sharding import PartitionSpec as P
+
 
 EPS = 1e-06
 F32 = jnp.float32
@@ -66,18 +69,6 @@
     return copies
 
 
-def rims_kernel(x_ref, w_ref, r_ref, i_ref, v_ref, out_ref, rows_ref, sems):
-    at = 0
-    pairs = []
-    for ref in (x_ref, w_ref, r_ref, i_ref, v_ref):
-        length, width = ref.shape[1:]
-        pairs.append((ref.at[0, pl.ds(length - PAD, PAD)], rows_ref.at[:, pl.ds(at, width)]))
-        at += width
-    for copy in fetch(pairs, sems):
-        copy.wait()
-    out_ref[...] = rows_ref[PAD - RIM :, :]
-
-
 def filtered(rows, taps, rim, pad_ref):
     length, width = rows.shape
     span = taps.shape[0]
@@ -102,9 +93,9 @@
 
 def prepare_kernel(
     x_hbm, w_hbm, r_hbm, i_hbm, v_hbm, o_hbm, gate_hbm, xt_hbm, wt_hbm, rt_hbm, ct_hbm, scale_hbm,
-    step_hbm, spike_hbm, off_hbm, rate_hbm,
+    step_hbm, spike_hbm, off_hbm, rate_hbm, s_hbm, c_hbm,
     weighted_ref, writes_ref, reads_ref, inside_ref, conv_ref, open_ref, head_ref,
-    xt_ref, wt_ref, rt_ref, ct_ref, scale_ref, dt_ref, rise_ref, remain_ref,
+    xt_ref, wt_ref, rt_ref, ct_ref, scale_ref, dt_ref, rise_ref, remain_ref, both_ref, rim_ref,
     x_ref, w_ref, r_ref, i_ref, v_ref, o_ref, gate_ref,
     step_ref, spike_ref, off_ref, rate_ref, pad_ref, sems,
 ):
@@ -129,6 +120,8 @@
             (o_hbm.at[0], o_ref),
             (ct_hbm, ct_ref),
             (scale_hbm, scale_ref),
+            (s_hbm, both_ref.at[pl.ds(0, s_hbm.shape[0])]),
+            (c_hbm, both_ref.at[pl.ds(s_hbm.shape[0], c_hbm.shape[0])]),
         ),
         sems,
     )
@@ -203,6 +196,8 @@
     at = 0
     for ref in (x_ref, w_ref, r_ref, i_ref, v_ref, o_ref):
         head_ref[:, at : at + ref.shape[1]] = ref[0:HEAD, :]
+        if ref is not o_ref:
+            rim_ref[:, at : at + ref.shape[1]] = ref[length - RIM : length, :]
         at += ref.shape[1]
 
 
@@ -319,7 +314,6 @@
     per_group = width // LANES // groups
     kept = jnp.exp(rise_ref[...])
     blocks = STATE // 16
-    copies = out_ref.shape[0]
     for g in range(groups):
         read = reads_ref[:, g * STATE : (g + 1) * STATE]
         squares = jnp.zeros((length, LANES), F32)
@@ -338,43 +332,42 @@
         for k, q in enumerate(range(g * per_group, (g + 1) * per_group)):
             cols = slice(q * LANES, (q + 1) * LANES)
             value = (gated[k] * inverse * scale_ref[:, cols]).astype(BF16)
-            for c in range(copies):
-                out_ref[c, :, cols] = value
-    for c in range(copies):
-        out_ref[c, :, width:] = conv_ref[...]
-
-
-def project_kernel(half_ref, a_ref, s_ref, c_ref, out_ref):
-    seqs, length, depth = a_ref.shape
-    width = s_ref.shape[0]
-    start = half_ref[0]
-    for k in range(seqs // 2):
-        rows = a_ref[start + k]
-        out_ref[k] = (
-            jnp.dot(rows[:, :width], s_ref[...], preferred_element_type=F32)
-            + jnp.dot(rows[:, width:], c_ref[...], preferred_element_type=F32)
-        ).astype(out_ref.dtype)
-
-
-def project(half, rows, s, c, dtype):
-    seqs, length, _ = rows.shape
-    out = jax.ShapeDtypeStruct((seqs // 2, length, s.shape[1]), dtype)
-    ins = (half, rows, s, c)
-    return pl.pallas_call(
-        project_kernel,
-        grid=(1,),
-        in_specs=[pl.BlockSpec(memory_space=pltpu.SMEM)] + [whole(a.shape) for a in ins[1:]],
-        out_specs=whole(out.shape),
-        out_shape=out,
-        compiler_params=pltpu.CompilerParams(vmem_limit_bytes=24 * 1024 * 1024),
-        cost_estimate=pl.CostEstimate(
-            flops=400_000_000, bytes_accessed=2_000_000, transcendentals=0
-        ),
-    )(*ins)
-
-
-def merge_kernel(kept_ref, got_ref, out_ref):
-    out_ref[...] = (kept_ref[...] + got_ref[...].astype(F32)).astype(BF16)
+            out_ref[:, cols] = value
+    out_ref[:, width:] = conv_ref[...]
+
+
+def far_kernel(a_ref, w_ref, out_ref):
+    out_ref[...] = jnp.dot(a_ref[...], w_ref[...], preferred_element_type=F32).astype(BF16)
+
+
+def part_kernel(kept, early, first_ref, second_ref, w_ref, out_ref):
+    core = lax.axis_index("tp")
+    chip = lax.axis_index("fs")
+    odd = lax.rem(chip, 2)
+    seq = 2 * (core if kept else 1 - core) + (odd if early else 1 - odd)
+    away = lax.rem(seq - chip + 4, 4)
+
+    @pl.when(away < 2)
+    def _():
+        out_ref[...] = jnp.dot(first_ref[...], w_ref[...], preferred_element_type=F32).astype(out_ref.dtype)
+
+    @pl.when(away >= 2)
+    def _():
+        if early:
+            out_ref[...] = second_ref[...].astype(out_ref.dtype)
+        else:
+            out_ref[...] = jnp.dot(second_ref[...], w_ref[...], preferred_element_type=F32).astype(out_ref.dtype)
+
+
+def part(kept, early, first, second, rows):
+    out = jax.ShapeDtypeStruct((first.shape[0], rows.shape[1]), F32 if kept else BF16)
+    return call(functools.partial(part_kernel, kept, early), [out], (first, second, rows))[0]
+
+
+def merge_kernel(early_ref, early_got_ref, late_ref, late_got_ref, out_ref):
+    odd = lax.rem(lax.axis_index("fs"), 2)
+    out_ref[odd] = (early_ref[...] + early_got_ref[...].astype(F32)).astype(BF16)
+    out_ref[1 - odd] = (late_ref[...] + late_got_ref[...].astype(F32)).astype(BF16)
 
 
 def per_device(
@@ -412,15 +405,11 @@
         convolution_value_rows,
     )
     all_width = sum(a.shape[2] for a in ends)
-    rims = call(
-        rims_kernel, [sds((RIM, all_width), BF16)], ends, 5, [vmem((PAD, all_width), BF16), sems(5)], 1000
-    )[0]
-    before = lax.ppermute(rims, "sp", [(k, k + 1) for k in range(members - 1)])
     ins = (
         *ends, convolution_outer_gate, output_gate_logits,
         head_input_taps, state_input_taps, readout_filter_taps, gated_filter_taps,
         grouped_norm_scale[None], jnp.swapaxes(step_logits, 1, 2), decay_extra_spikes.T,
-        head_step_offset[None], head_decay_logrates[None],
+        head_step_offset[None], head_decay_logrates[None], state_output_rows, convolution_output_rows,
     )
     tall = sds((length, width), BF16)
     slim = sds((length, narrow), BF16)
@@ -431,6 +420,7 @@
         sds(head_input_taps.shape, BF16), sds(state_input_taps.shape, BF16),
         sds(readout_filter_taps.shape, BF16), sds(gated_filter_taps.shape, BF16),
         sds((1, width), F32), sds((HEAD, heads), F32), sds((length, heads), F32), sds((HEAD, heads), F32),
+        sds((width + wide, state_output_rows.shape[1]), BF16), sds((RIM, all_width), BF16),
     ]
     pad = vmem((PAD + length, LANES))
     scratch = [vmem(a.shape[1:], BF16) for a in ins[:7]] + [
@@ -439,31 +429,42 @@
         vmem((1, heads)),
         vmem((1, heads)),
         pad,
-        sems(16),
+        sems(18),
     ]
     (
         weighted, writes, reads, inside, conv, opened, head, xt, wt, rt, ct, scale, dt, rise, remain,
-    ) = call(prepare_kernel, outs, ins, 16, scratch)
+        rows_own, rims,
+    ) = call(prepare_kernel, outs, ins, 18, scratch)
+    before = lax.ppermute(rims, "sp", [(k, k + 1) for k in range(members - 1)])
     ins = (before, weighted, writes, reads, inside, conv, head, xt, wt, rt, ct, dt, rise, remain)
     outs = [sds((members, 16 + EXTRA, LANES), BF16), slim, full, side]
     payload, reads, inside, conv = call(state_kernel, outs, ins, 0, [pad])
-    core = lax.axis_index("tp")
     seqs = copies
-    mine = (core * (seqs // 2)).astype(jnp.int32)[None]
-    theirs = ((1 - core) * (seqs // 2)).astype(jnp.int32)[None]
-    payload, mine, theirs = lax.optimization_barrier((payload, mine, theirs))
+
+    def moved(value, away):
+        return lax.ppermute(value, "fs", [(k, (k + away) % seqs) for k in range(seqs)])
+
+    rows_far = moved(rows_own, 2)
     gathered = lax.all_to_all(
         payload, "sp", 0, 0, axis_index_groups=turned(members, FIRST_OUT), tiled=True
     )
     prefixes = call(scan_kernel, [sds((members, 16, LANES), BF16)], (gathered,))[0]
     incoming = lax.all_to_all(prefixes, "sp", 0, 0, axis_index_groups=turned(members, FIRST_BACK), tiled=True)
     ins = (incoming, reads, rise, inside, opened, scale, conv)
-    joined = call(gate_kernel, [sds((copies, length, width + wide), BF16)], ins)[0]
-    rows = lax.all_to_all(joined, "fs", 0, 0, tiled=True)
-    sent = project(theirs, rows, state_output_rows, convolution_output_rows, BF16)
-    got = lax.ppermute(sent, "tp", [(0, 1), (1, 0)])
-    kept = project(mine, rows, state_output_rows, convolution_output_rows, F32)
-    return call(merge_kernel, [sds(got.shape, BF16)], (kept, got))[0]
+    own = call(gate_kernel, [sds((length, width + wide), BF16)], ins)[0]
+    last = moved(own, 1)
+    following = moved(own, -1)
+    partial = call(far_kernel, [sds((length, rows_own.shape[1]), BF16)], (own, rows_far))[0]
+    far = moved(partial, 2)
+    swap = [(0, 1), (1, 0)]
+    sent = part(False, True, own, far, rows_own)
+    early_got = lax.ppermute(sent, "tp", swap)
+    early = part(True, True, own, far, rows_own)
+    sent = part(False, False, following, last, rows_own)
+    late_got = lax.ppermute(sent, "tp", swap)
+    late = part(True, False, following, last, rows_own)
+    out = sds((2, length, rows_own.shape[1]), BF16)
+    return call(merge_kernel, [out], (early, early_got, late, late_got))[0]
 
 
 def solution(mesh):

time: 86.5 us -> 85.5 us (0.988)
  blocking collectives: 68.7 us -> 46.2 us
  starting transfers between devices: 9.29 us -> 26.6 us
  waiting for transfers between devices: 0.55 us -> 5.02 us
    all_to_all x1 -> x0, blocking collectives: 22.1 us -> none  [per_device(): rows = lax.all_to_all(joined, 'fs', 0, 0, tiled=True)]
    ppermute x1 -> x6, starting transfers between devices: 5.27 us -> 22.6 us  [the longest x4 13.1 us: moved(): lax.ppermute(value, 'fs', [(k, (k + away) % seqs) for k in range(seqs)])]
    ppermute x1 -> x6, waiting for transfers between devices: 0.55 us -> 5.02 us  [the longest x4 4.16 us: moved(): lax.ppermute(value, 'fs', [(k, (k + away) % seqs) for k in range(seqs)])]
    pallas_call x2 -> x0, Pallas kernels: 1.16 us -> none  [project(): pl.pallas_call(project_kernel, grid=(1,), in_specs=[pl.BlockSpec(memory_s...]
    pallas_call x6 -> x10, Pallas kernels: 6.25 us -> 6.92 us  [call(): pl.pallas_call(kernel, grid=(1,), in_specs=[HBM] * far + [whole(a.shape)...]
  transfers between devices with their start and end apart: 2 -> 7, of which waited for: 1 -> 3; matrix products, arithmetic and copies ran while one was open for 0% -> 0% of each run, Pallas kernels for 4% -> 4%
where the time goes in v3:
time: 85.5 us; the launch traced here: 84.9 us
  blocking collectives  46.2 us (54%)
  starting transfers between devices  26.6 us (31%)
  Pallas kernels  6.92 us (8%)
  waiting for transfers between devices  5.02 us (6%)
    all_to_all x1, blocking collectives, per_device(): lax.all_to_all(payload, 'sp', 0, 0, axis_index_groups=turned(members, FIR...  28 us
    all_to_all x1, blocking collectives, per_device(): lax.all_to_all(prefixes, 'sp', 0, 0, axis_index_groups=turned(members, FI...  18.2 us
    ppermute x4, starting transfers between devices, moved(): lax.ppermute(value, 'fs', [(k, (k + away) % seqs) for k in range(seqs)])  13.1 us
    ppermute x1, starting transfers between devices, per_device(): late_got = lax.ppermute(sent, 'tp', swap)  7.58 us
    pallas_call x10, Pallas kernels, call(): pl.pallas_call(kernel, grid=(1,), in_specs=[HBM] * far + [whole(a.shape)...  6.92 us
    ppermute x4, waiting for transfers between devices, moved(): lax.ppermute(value, 'fs', [(k, (k + away) % seqs) for k in range(seqs)])  4.16 us
    ppermute x1, starting transfers between devices, per_device(): before = lax.ppermute(rims, 'sp', [(k, k + 1) for k in range(members - 1)])  4.02 us
    ppermute x1, starting transfers between devices, per_device(): early_got = lax.ppermute(sent, 'tp', swap)  1.92 us
  transfers between devices with their start and end apart: 7, of which 3 were waited for; matrix products, arithmetic and copies ran while one was open for 0% of the time, Pallas kernels for 4%

profile of v3, /device:TPU:1, one launch (start us, length us, event | category | flops | bytes accessed | tf_op | source)
XLA Modules:
  0.0 84.9 jit_solution(174869201097840830)
XLA Ops:
  0.0 3.0 %shard_map.172 = (bf16[128,1024]{1,0:T(8,128)(2,1)S(1)}, bf16[128,256]{1,0:T(8,128)(2,1)S(1)}, bf16[128,256]{1,0:T(8,128)(2,1)S(1)}, f32[128,1024]{1,0:T(8,128)S...) custom-call(bf16[1,128,1024]{2,1,0:T(8,128)(2,1)} %x_hbm.1, ...), custom_call_target="tpu_custom_call" | custom-call | flops 50000000 | bytes 2000000 | tf_op jit(solution)/shard_map/pallas_call | solution.py:34
  3.0 4.0 %collective-permute-start = (bf16[4,2560]{1,0:T(4,128)(2,1)S(1)}, bf16[4,2560]{1,0:T(4,128)(2,1)S(1)}, u32[]{:S(2)}, u32[]{:S(2)}) collective-permute-start(bf16[4,2560]{1,0:T(4,128)(2,1)S(1)} %get-tuple-element.26), channel_id=1, source_target_pairs={{0,8},{8,16},{16,24},{24,32},{32,40},{40,48},{48,56},{56,64},{64,7... | collective-permute-start | bytes 61448 | tf_op jit(solution)/shard_map/ppermute | solution.py:438
  7.0 4.7 %collective-permute-start.1 = (bf16[1536,512]{1,0:T(8,128)(2,1)S(1)}, bf16[1536,512]{1,0:T(8,128)(2,1)S(1)}, u32[]{:S(2)}, u32[]{:S(2)}) collective-permute-start(bf16[1536,512]{1,0:T(8,128)(2,1)S(1)} %get-tuple-element.46.w_ref), channel_id=1, source_target_pairs={{0,4},{2,6},{4,0},{6,2},{1,5},{3,7},{5,1},{7,3},{8,12},{10,14},{12... | collective-permute-start | bytes 4718600 | tf_op jit(solution)/shard_map/ppermute | solution.py:445
  11.7 0.0 collective-permute-done.rim_ref
  11.7 0.9 %shard_map.173 = (bf16[64,24,128]{2,1,0:T(8,128)(2,1)S(1)}, bf16[128,256]{1,0:T(8,128)(2,1)S(1)}, f32[128,1024]{1,0:T(8,128)S(1)}, bf16[128,512]{1,0:T(8,128)(2,1)S(1)}) custom-call(bf16[4,2560]{1,0:T(4,128)(2,1)S(1)} %collective-permute-done.rim_ref, bf16[128,1024]{1,0:T(8,128)(2,1)S(1)} %get-tuple-element.27.weighted_ref, ...), custom_call_target="tpu_custom_call" | custom-call | flops 50000000 | bytes 2000000 | tf_op jit(solution)/shard_map/pallas_call | solution.py:34
  12.5 28.0 %all_to_all.10.in_ref = bf16[64,24,128]{2,1,0:T(8,128)(2,1)S(1)} all-to-all(bf16[64,24,128]{2,1,0:T(8,128)(2,1)S(1)} %get-tuple-element.40), channel_id=1, replica_groups={{416,424,432,440,448,456,464,472,480,488,496,504,0,8,16,24,32,40,48,56,..., dimensions={0} | all-to-all | bytes 786432 | tf_op jit(solution)/shard_map/all_to_all | solution.py:448
  40.5 0.1 shard_map.174
  40.7 18.2 %all_to_all.11.p_ref = bf16[64,16,128]{2,1,0:T(8,128)(2,1)S(1)} all-to-all(bf16[64,16,128]{2,1,0:T(8,128)(2,1)S(1)} %shard_map.174), channel_id=1, replica_groups={{416,424,432,440,448,456,464,472,480,488,496,504,0,8,16,24,32,40,48,56,..., dimensions={0} | all-to-all | bytes 524288 | tf_op jit(solution)/shard_map/all_to_all | solution.py:452
  58.9 0.6 shard_map.175.a_ref.first_ref
  59.5 2.2 %collective-permute-start.5 = (bf16[128,1536]{1,0:T(8,128)(2,1)S(1)}, bf16[128,1536]{1,0:T(8,128)(2,1)S(1)}, u32[]{:S(2)}, u32[]{:S(2)}) collective-permute-start(bf16[128,1536]{1,0:T(8,128)(2,1)S(1)} %shard_map.175.a_ref.first_ref), channel_id=1, source_target_pairs={{0,2},{2,4},{4,6},{6,0},{1,3},{3,5},{5,7},{7,1},{8,10},{10,12},{12... | collective-permute-start | bytes 1179656 | tf_op jit(solution)/shard_map/ppermute | solution.py:445
  61.7 4.3 %collective-permute-start.4 = (bf16[128,1536]{1,0:T(8,128)(2,1)S(1)}, bf16[128,1536]{1,0:T(8,128)(2,1)S(1)}, u32[]{:S(2)}, u32[]{:S(2)}) collective-permute-start(bf16[128,1536]{1,0:T(8,128)(2,1)S(1)} %shard_map.175.a_ref.first_ref), channel_id=1, source_target_pairs={{0,6},{2,0},{4,2},{6,4},{1,7},{3,1},{5,3},{7,5},{8,14},{10,8},{12,... | collective-permute-start | bytes 1179656 | tf_op jit(solution)/shard_map/ppermute | solution.py:445
  66.0 0.0 collective-permute-done.1.w_ref
  66.0 0.4 shard_map.176
  66.4 1.9 %collective-permute-start.2 = (bf16[128,512]{1,0:T(8,128)(2,1)S(1)}, bf16[128,512]{1,0:T(8,128)(2,1)S(1)}, u32[]{:S(2)}, u32[]{:S(2)}) collective-permute-start(bf16[128,512]{1,0:T(8,128)(2,1)S(1)} %shard_map.176), channel_id=1, source_target_pairs={{0,4},{2,6},{4,0},{6,2},{1,5},{3,7},{5,1},{7,3},{8,12},{10,14},{12... | collective-permute-start | bytes 393224 | tf_op jit(solution)/shard_map/ppermute | solution.py:445
  68.3 2.6 %collective-permute-done.5.second_ref = bf16[128,1536]{1,0:T(8,128)(2,1)S(1)} collective-permute-done((bf16[128,1536]{1,0:T(8,128)(2,1)S(1)}, bf16[128,1536]{1,0:T(8,128)(2,1)S(1)}, u32[]{:S(2)}, u32[]{:S(2)}) %collective-permute-start.5) | collective-permute-done | bytes 393248 | tf_op jit(solution)/shard_map/ppermute | solution.py:445
  70.9 1.6 %collective-permute-done.4.first_ref = bf16[128,1536]{1,0:T(8,128)(2,1)S(1)} collective-permute-done((bf16[128,1536]{1,0:T(8,128)(2,1)S(1)}, bf16[128,1536]{1,0:T(8,128)(2,1)S(1)}, u32[]{:S(2)}, u32[]{:S(2)}) %collective-permute-start.4) | collective-permute-done | bytes 393248 | tf_op jit(solution)/shard_map/ppermute | solution.py:445
  72.5 0.4 shard_map.180
  72.9 7.6 %collective-permute-start.6 = (bf16[128,512]{1,0:T(8,128)(2,1)S(1)}, bf16[128,512]{1,0:T(8,128)(2,1)S(1)}, u32[]{:S(2)}, u32[]{:S(2)}) collective-permute-start(bf16[128,512]{1,0:T(8,128)(2,1)S(1)} %shard_map.180), channel_id=1, source_target_pairs={{0,1},{1,0},{2,3},{3,2},{4,5},{5,4},{6,7},{7,6},{8,9},{9,8},{10,11... | collective-permute-start | bytes 393224 | tf_op jit(solution)/shard_map/ppermute | solution.py:464
  80.4 0.0 collective-permute-done.2.second_ref
  80.5 0.4 shard_map.178
  80.9 1.9 %collective-permute-start.3 = (bf16[128,512]{1,0:T(8,128)(2,1)S(1)}, bf16[128,512]{1,0:T(8,128)(2,1)S(1)}, u32[]{:S(2)}, u32[]{:S(2)}) collective-permute-start(bf16[128,512]{1,0:T(8,128)(2,1)S(1)} %shard_map.178), channel_id=1, source_target_pairs={{0,1},{1,0},{2,3},{3,2},{4,5},{5,4},{6,7},{7,6},{8,9},{9,8},{10,11... | collective-permute-start | bytes 393224 | tf_op jit(solution)/shard_map/ppermute | solution.py:461
  82.8 0.4 shard_map.179.late_ref
  83.2 0.0 collective-permute-done.6.late_got_ref
  83.3 0.9 %collective-permute-done.3.early_got_ref = bf16[128,512]{1,0:T(8,128)(2,1)S(1)} collective-permute-done((bf16[128,512]{1,0:T(8,128)(2,1)S(1)}, bf16[128,512]{1,0:T(8,128)(2,1)S(1)}, u32[]{:S(2)}, u32[]{:S(2)}) %collective-permute-start.3) | collective-permute-done | bytes 131104 | tf_op jit(solution)/shard_map/ppermute | solution.py:461
  84.1 0.7 shard_map.181
  (1 shorter events, 0.0 us)
Async XLA Ops:
  3.0 8.7 %collective-permute-start = (bf16[4,2560]{1,0:T(4,128)(2,1)S(1)}, bf16[4,2560]{1,0:T(4,128)(2,1)S(1)}, u32[]{:S(2)}, u32[]{:S(2)}) collective-permute-start(bf16[4,2560]{1,0:T(4,128)(2,1)S(1)} %get-tuple-element.26), channel_id=1, source_target_pairs={{0,8},{8,16},{16,24},{24,32},{32,40},{40,48},{48,56},{56,64},{64,7... | collective-permute-start | bytes 61448 | tf_op jit(solution)/shard_map/ppermute | solution.py:438
  7.0 59.0 %collective-permute-start.1 = (bf16[1536,512]{1,0:T(8,128)(2,1)S(1)}, bf16[1536,512]{1,0:T(8,128)(2,1)S(1)}, u32[]{:S(2)}, u32[]{:S(2)}) collective-permute-start(bf16[1536,512]{1,0:T(8,128)(2,1)S(1)} %get-tuple-element.46.w_ref), channel_id=1, source_target_pairs={{0,4},{2,6},{4,0},{6,2},{1,5},{3,7},{5,1},{7,3},{8,12},{10,14},{12... | collective-permute-start | bytes 4718600 | tf_op jit(solution)/shard_map/ppermute | solution.py:445
  59.5 11.4 %collective-permute-start.5 = (bf16[128,1536]{1,0:T(8,128)(2,1)S(1)}, bf16[128,1536]{1,0:T(8,128)(2,1)S(1)}, u32[]{:S(2)}, u32[]{:S(2)}) collective-permute-start(bf16[128,1536]{1,0:T(8,128)(2,1)S(1)} %shard_map.175.a_ref.first_ref), channel_id=1, source_target_pairs={{0,2},{2,4},{4,6},{6,0},{1,3},{3,5},{5,7},{7,1},{8,10},{10,12},{12... | collective-permute-start | bytes 1179656 | tf_op jit(solution)/shard_map/ppermute | solution.py:445
  61.7 10.8 %collective-permute-start.4 = (bf16[128,1536]{1,0:T(8,128)(2,1)S(1)}, bf16[128,1536]{1,0:T(8,128)(2,1)S(1)}, u32[]{:S(2)}, u32[]{:S(2)}) collective-permute-start(bf16[128,1536]{1,0:T(8,128)(2,1)S(1)} %shard_map.175.a_ref.first_ref), channel_id=1, source_target_pairs={{0,6},{2,0},{4,2},{6,4},{1,7},{3,1},{5,3},{7,5},{8,14},{10,8},{12,... | collective-permute-start | bytes 1179656 | tf_op jit(solution)/shard_map/ppermute | solution.py:445
  66.4 14.1 %collective-permute-start.2 = (bf16[128,512]{1,0:T(8,128)(2,1)S(1)}, bf16[128,512]{1,0:T(8,128)(2,1)S(1)}, u32[]{:S(2)}, u32[]{:S(2)}) collective-permute-start(bf16[128,512]{1,0:T(8,128)(2,1)S(1)} %shard_map.176), channel_id=1, source_target_pairs={{0,4},{2,6},{4,0},{6,2},{1,5},{3,7},{5,1},{7,3},{8,12},{10,14},{12... | collective-permute-start | bytes 393224 | tf_op jit(solution)/shard_map/ppermute | solution.py:445
  72.9 10.4 %collective-permute-start.6 = (bf16[128,512]{1,0:T(8,128)(2,1)S(1)}, bf16[128,512]{1,0:T(8,128)(2,1)S(1)}, u32[]{:S(2)}, u32[]{:S(2)}) collective-permute-start(bf16[128,512]{1,0:T(8,128)(2,1)S(1)} %shard_map.180), channel_id=1, source_target_pairs={{0,1},{1,0},{2,3},{3,2},{4,5},{5,4},{6,7},{7,6},{8,9},{9,8},{10,11... | collective-permute-start | bytes 393224 | tf_op jit(solution)/shard_map/ppermute | solution.py:464
  80.9 3.2 %collective-permute-start.3 = (bf16[128,512]{1,0:T(8,128)(2,1)S(1)}, bf16[128,512]{1,0:T(8,128)(2,1)S(1)}, u32[]{:S(2)}, u32[]{:S(2)}) collective-permute-start(bf16[128,512]{1,0:T(8,128)(2,1)S(1)} %shard_map.178), channel_id=1, source_target_pairs={{0,1},{1,0},{2,3},{3,2},{4,5},{5,4},{6,7},{7,6},{8,9},{9,8},{10,11... | collective-permute-start | bytes 393224 | tf_op jit(solution)/shard_map/ppermute | solution.py:461

commit v4 on v3

--- a/solution.py
+++ b/solution.py
@@ -19,7 +19,7 @@
 RIM = 4
 HEAD = 16
 FIRST_OUT = 52
-FIRST_BACK = 52
+FIRST_BACK = 60
 
 
 def whole(shape):
@@ -60,6 +60,21 @@
     first = jnp.broadcast_to(cols[:, 2 * q : 2 * q + 1], (rows, LANES))
     second = jnp.broadcast_to(cols[:, 2 * q + 1 : 2 * q + 2], (rows, LANES))
     return jnp.where(low, first, second)
+
+
+def three(cols):
+    high = cols.astype(BF16)
+    rest = cols - high.astype(F32)
+    middle = rest.astype(BF16)
+    return jnp.concatenate([high, middle, (rest - middle.astype(F32)).astype(BF16)], axis=1)
+
+
+def spread(parts, first, lanes, width):
+    heads = parts.shape[1] // 3
+    shape = (parts.shape[1], width)
+    wanted = first + (lax.broadcasted_iota(jnp.int32, shape, 1) >> (lanes.bit_length() - 1))
+    chosen = (lax.broadcasted_iota(jnp.int32, shape, 0) & (heads - 1)) == wanted
+    return jnp.dot(parts, chosen.astype(BF16), preferred_element_type=F32)
 
 
 def fetch(pairs, sems):
@@ -312,7 +327,7 @@
     length, width = inside_ref.shape
     groups = reads_ref.shape[1] // STATE
     per_group = width // LANES // groups
-    kept = jnp.exp(rise_ref[...])
+    kept = three(jnp.exp(rise_ref[...]))
     blocks = STATE // 16
     for g in range(groups):
         read = reads_ref[:, g * STATE : (g + 1) * STATE]
@@ -323,7 +338,7 @@
             spots = [(q * blocks + k + FIRST_OUT - FIRST_BACK) % p_ref.shape[0] for k in range(blocks)]
             before = jnp.concatenate([p_ref[spot] for spot in spots], axis=0)
             carried = jnp.dot(read, before, preferred_element_type=F32)
-            y = inside_ref[:, cols] + carried * pair_lanes(kept, q, length)
+            y = inside_ref[:, cols] + carried * spread(kept, 2 * q, HEAD_DIM, LANES)
             y = y * open_ref[:, cols]
             squares = squares + y * y
             gated.append(y)

time: 85.5 us -> 84.7 us (level)
  no operation moved by 1% of the time
where the time goes in v4:
time: 84.7 us; the launch traced here: 84.3 us
  blocking collectives  45.7 us (54%)
  starting transfers between devices  26.8 us (32%)
  Pallas kernels  6.78 us (8%)
  waiting for transfers between devices  4.76 us (6%)
    all_to_all x1, blocking collectives, per_device(): lax.all_to_all(payload, 'sp', 0, 0, axis_index_groups=turned(members, FIR...  28 us
    all_to_all x1, blocking collectives, per_device(): lax.all_to_all(prefixes, 'sp', 0, 0, axis_index_groups=turned(members, FI...  17.8 us
    ppermute x4, starting transfers between devices, moved(): lax.ppermute(value, 'fs', [(k, (k + away) % seqs) for k in range(seqs)])  13.1 us
    ppermute x1, starting transfers between devices, per_device(): late_got = lax.ppermute(sent, 'tp', swap)  7.84 us
    pallas_call x10, Pallas kernels, call(): pl.pallas_call(kernel, grid=(1,), in_specs=[HBM] * far + [whole(a.shape)...  6.78 us
    ppermute x1, starting transfers between devices, per_device(): before = lax.ppermute(rims, 'sp', [(k, k + 1) for k in range(members - 1)])  4.02 us
    ppermute x4, waiting for transfers between devices, moved(): lax.ppermute(value, 'fs', [(k, (k + away) % seqs) for k in range(seqs)])  3.9 us
    ppermute x1, starting transfers between devices, per_device(): early_got = lax.ppermute(sent, 'tp', swap)  1.92 us
  transfers between devices with their start and end apart: 7, of which 3 were waited for; matrix products, arithmetic and copies ran while one was open for 0% of the time, Pallas kernels for 4%

profile of v4, /device:TPU:1, one launch (start us, length us, event | category | flops | bytes accessed | tf_op | source)
XLA Modules:
  0.0 84.3 jit_solution(6219677357065712438)
XLA Ops:
  0.0 3.0 %shard_map.172 = (bf16[128,1024]{1,0:T(8,128)(2,1)S(1)}, bf16[128,256]{1,0:T(8,128)(2,1)S(1)}, bf16[128,256]{1,0:T(8,128)(2,1)S(1)}, f32[128,1024]{1,0:T(8,128)S...) custom-call(bf16[1,128,1024]{2,1,0:T(8,128)(2,1)} %x_hbm.1, ...), custom_call_target="tpu_custom_call" | custom-call | flops 50000000 | bytes 2000000 | tf_op jit(solution)/shard_map/pallas_call | solution.py:34
  3.0 4.0 %collective-permute-start = (bf16[4,2560]{1,0:T(4,128)(2,1)S(1)}, bf16[4,2560]{1,0:T(4,128)(2,1)S(1)}, u32[]{:S(2)}, u32[]{:S(2)}) collective-permute-start(bf16[4,2560]{1,0:T(4,128)(2,1)S(1)} %get-tuple-element.26), channel_id=1, source_target_pairs={{0,8},{8,16},{16,24},{24,32},{32,40},{40,48},{48,56},{56,64},{64,7... | collective-permute-start | bytes 61448 | tf_op jit(solution)/shard_map/ppermute | solution.py:453
  7.0 4.7 %collective-permute-start.1 = (bf16[1536,512]{1,0:T(8,128)(2,1)S(1)}, bf16[1536,512]{1,0:T(8,128)(2,1)S(1)}, u32[]{:S(2)}, u32[]{:S(2)}) collective-permute-start(bf16[1536,512]{1,0:T(8,128)(2,1)S(1)} %get-tuple-element.46.w_ref), channel_id=1, source_target_pairs={{0,4},{2,6},{4,0},{6,2},{1,5},{3,7},{5,1},{7,3},{8,12},{10,14},{12... | collective-permute-start | bytes 4718600 | tf_op jit(solution)/shard_map/ppermute | solution.py:460
  11.7 0.0 collective-permute-done.rim_ref
  11.7 0.9 %shard_map.173 = (bf16[64,24,128]{2,1,0:T(8,128)(2,1)S(1)}, bf16[128,256]{1,0:T(8,128)(2,1)S(1)}, f32[128,1024]{1,0:T(8,128)S(1)}, bf16[128,512]{1,0:T(8,128)(2,1)S(1)}) custom-call(bf16[4,2560]{1,0:T(4,128)(2,1)S(1)} %collective-permute-done.rim_ref, bf16[128,1024]{1,0:T(8,128)(2,1)S(1)} %get-tuple-element.27.weighted_ref, ...), custom_call_target="tpu_custom_call" | custom-call | flops 50000000 | bytes 2000000 | tf_op jit(solution)/shard_map/pallas_call | solution.py:34
  12.5 28.0 %all_to_all.10.in_ref = bf16[64,24,128]{2,1,0:T(8,128)(2,1)S(1)} all-to-all(bf16[64,24,128]{2,1,0:T(8,128)(2,1)S(1)} %get-tuple-element.40), channel_id=1, replica_groups={{416,424,432,440,448,456,464,472,480,488,496,504,0,8,16,24,32,40,48,56,..., dimensions={0} | all-to-all | bytes 786432 | tf_op jit(solution)/shard_map/all_to_all | solution.py:463
  40.5 0.1 shard_map.174
  40.7 17.8 %all_to_all.11.p_ref = bf16[64,16,128]{2,1,0:T(8,128)(2,1)S(1)} all-to-all(bf16[64,16,128]{2,1,0:T(8,128)(2,1)S(1)} %shard_map.174), channel_id=1, replica_groups={{480,488,496,504,0,8,16,24,32,40,48,56,64,72,80,88,96,104,112,120,128,1..., dimensions={0} | all-to-all | bytes 524288 | tf_op jit(solution)/shard_map/all_to_all | solution.py:467
  58.4 0.5 shard_map.175.a_ref.first_ref
  58.9 2.2 %collective-permute-start.5 = (bf16[128,1536]{1,0:T(8,128)(2,1)S(1)}, bf16[128,1536]{1,0:T(8,128)(2,1)S(1)}, u32[]{:S(2)}, u32[]{:S(2)}) collective-permute-start(bf16[128,1536]{1,0:T(8,128)(2,1)S(1)} %shard_map.175.a_ref.first_ref), channel_id=1, source_target_pairs={{0,2},{2,4},{4,6},{6,0},{1,3},{3,5},{5,7},{7,1},{8,10},{10,12},{12... | collective-permute-start | bytes 1179656 | tf_op jit(solution)/shard_map/ppermute | solution.py:460
  61.2 4.3 %collective-permute-start.4 = (bf16[128,1536]{1,0:T(8,128)(2,1)S(1)}, bf16[128,1536]{1,0:T(8,128)(2,1)S(1)}, u32[]{:S(2)}, u32[]{:S(2)}) collective-permute-start(bf16[128,1536]{1,0:T(8,128)(2,1)S(1)} %shard_map.175.a_ref.first_ref), channel_id=1, source_target_pairs={{0,6},{2,0},{4,2},{6,4},{1,7},{3,1},{5,3},{7,5},{8,14},{10,8},{12,... | collective-permute-start | bytes 1179656 | tf_op jit(solution)/shard_map/ppermute | solution.py:460
  65.4 0.0 collective-permute-done.1.w_ref
  65.4 0.4 shard_map.176
  65.8 1.9 %collective-permute-start.2 = (bf16[128,512]{1,0:T(8,128)(2,1)S(1)}, bf16[128,512]{1,0:T(8,128)(2,1)S(1)}, u32[]{:S(2)}, u32[]{:S(2)}) collective-permute-start(bf16[128,512]{1,0:T(8,128)(2,1)S(1)} %shard_map.176), channel_id=1, source_target_pairs={{0,4},{2,6},{4,0},{6,2},{1,5},{3,7},{5,1},{7,3},{8,12},{10,14},{12... | collective-permute-start | bytes 393224 | tf_op jit(solution)/shard_map/ppermute | solution.py:460
  67.8 1.8 %collective-permute-done.5.second_ref = bf16[128,1536]{1,0:T(8,128)(2,1)S(1)} collective-permute-done((bf16[128,1536]{1,0:T(8,128)(2,1)S(1)}, bf16[128,1536]{1,0:T(8,128)(2,1)S(1)}, u32[]{:S(2)}, u32[]{:S(2)}) %collective-permute-start.5) | collective-permute-done | bytes 393248 | tf_op jit(solution)/shard_map/ppermute | solution.py:460
  69.6 2.1 %collective-permute-done.4.first_ref = bf16[128,1536]{1,0:T(8,128)(2,1)S(1)} collective-permute-done((bf16[128,1536]{1,0:T(8,128)(2,1)S(1)}, bf16[128,1536]{1,0:T(8,128)(2,1)S(1)}, u32[]{:S(2)}, u32[]{:S(2)}) %collective-permute-start.4) | collective-permute-done | bytes 393248 | tf_op jit(solution)/shard_map/ppermute | solution.py:460
  71.6 0.4 shard_map.180
  72.0 7.8 %collective-permute-start.6 = (bf16[128,512]{1,0:T(8,128)(2,1)S(1)}, bf16[128,512]{1,0:T(8,128)(2,1)S(1)}, u32[]{:S(2)}, u32[]{:S(2)}) collective-permute-start(bf16[128,512]{1,0:T(8,128)(2,1)S(1)} %shard_map.180), channel_id=1, source_target_pairs={{0,1},{1,0},{2,3},{3,2},{4,5},{5,4},{6,7},{7,6},{8,9},{9,8},{10,11... | collective-permute-start | bytes 393224 | tf_op jit(solution)/shard_map/ppermute | solution.py:479
  79.9 0.0 collective-permute-done.2.second_ref
  79.9 0.4 shard_map.178
  80.3 1.9 %collective-permute-start.3 = (bf16[128,512]{1,0:T(8,128)(2,1)S(1)}, bf16[128,512]{1,0:T(8,128)(2,1)S(1)}, u32[]{:S(2)}, u32[]{:S(2)}) collective-permute-start(bf16[128,512]{1,0:T(8,128)(2,1)S(1)} %shard_map.178), channel_id=1, source_target_pairs={{0,1},{1,0},{2,3},{3,2},{4,5},{5,4},{6,7},{7,6},{8,9},{9,8},{10,11... | collective-permute-start | bytes 393224 | tf_op jit(solution)/shard_map/ppermute | solution.py:476
  82.2 0.4 shard_map.179.late_ref
  82.7 0.0 collective-permute-done.6.late_got_ref
  82.7 0.9 %collective-permute-done.3.early_got_ref = bf16[128,512]{1,0:T(8,128)(2,1)S(1)} collective-permute-done((bf16[128,512]{1,0:T(8,128)(2,1)S(1)}, bf16[128,512]{1,0:T(8,128)(2,1)S(1)}, u32[]{:S(2)}, u32[]{:S(2)}) %collective-permute-start.3) | collective-permute-done | bytes 131104 | tf_op jit(solution)/shard_map/ppermute | solution.py:476
  83.5 0.7 shard_map.181
  (1 shorter events, 0.0 us)
Async XLA Ops:
  3.0 8.7 %collective-permute-start = (bf16[4,2560]{1,0:T(4,128)(2,1)S(1)}, bf16[4,2560]{1,0:T(4,128)(2,1)S(1)}, u32[]{:S(2)}, u32[]{:S(2)}) collective-permute-start(bf16[4,2560]{1,0:T(4,128)(2,1)S(1)} %get-tuple-element.26), channel_id=1, source_target_pairs={{0,8},{8,16},{16,24},{24,32},{32,40},{40,48},{48,56},{56,64},{64,7... | collective-permute-start | bytes 61448 | tf_op jit(solution)/shard_map/ppermute | solution.py:453
  7.0 58.4 %collective-permute-start.1 = (bf16[1536,512]{1,0:T(8,128)(2,1)S(1)}, bf16[1536,512]{1,0:T(8,128)(2,1)S(1)}, u32[]{:S(2)}, u32[]{:S(2)}) collective-permute-start(bf16[1536,512]{1,0:T(8,128)(2,1)S(1)} %get-tuple-element.46.w_ref), channel_id=1, source_target_pairs={{0,4},{2,6},{4,0},{6,2},{1,5},{3,7},{5,1},{7,3},{8,12},{10,14},{12... | collective-permute-start | bytes 4718600 | tf_op jit(solution)/shard_map/ppermute | solution.py:460
  58.9 10.6 %collective-permute-start.5 = (bf16[128,1536]{1,0:T(8,128)(2,1)S(1)}, bf16[128,1536]{1,0:T(8,128)(2,1)S(1)}, u32[]{:S(2)}, u32[]{:S(2)}) collective-permute-start(bf16[128,1536]{1,0:T(8,128)(2,1)S(1)} %shard_map.175.a_ref.first_ref), channel_id=1, source_target_pairs={{0,2},{2,4},{4,6},{6,0},{1,3},{3,5},{5,7},{7,1},{8,10},{10,12},{12... | collective-permute-start | bytes 1179656 | tf_op jit(solution)/shard_map/ppermute | solution.py:460
  61.2 10.5 %collective-permute-start.4 = (bf16[128,1536]{1,0:T(8,128)(2,1)S(1)}, bf16[128,1536]{1,0:T(8,128)(2,1)S(1)}, u32[]{:S(2)}, u32[]{:S(2)}) collective-permute-start(bf16[128,1536]{1,0:T(8,128)(2,1)S(1)} %shard_map.175.a_ref.first_ref), channel_id=1, source_target_pairs={{0,6},{2,0},{4,2},{6,4},{1,7},{3,1},{5,3},{7,5},{8,14},{10,8},{12,... | collective-permute-start | bytes 1179656 | tf_op jit(solution)/shard_map/ppermute | solution.py:460
  65.8 14.1 %collective-permute-start.2 = (bf16[128,512]{1,0:T(8,128)(2,1)S(1)}, bf16[128,512]{1,0:T(8,128)(2,1)S(1)}, u32[]{:S(2)}, u32[]{:S(2)}) collective-permute-start(bf16[128,512]{1,0:T(8,128)(2,1)S(1)} %shard_map.176), channel_id=1, source_target_pairs={{0,4},{2,6},{4,0},{6,2},{1,5},{3,7},{5,1},{7,3},{8,12},{10,14},{12... | collective-permute-start | bytes 393224 | tf_op jit(solution)/shard_map/ppermute | solution.py:460
  72.0 10.6 %collective-permute-start.6 = (bf16[128,512]{1,0:T(8,128)(2,1)S(1)}, bf16[128,512]{1,0:T(8,128)(2,1)S(1)}, u32[]{:S(2)}, u32[]{:S(2)}) collective-permute-start(bf16[128,512]{1,0:T(8,128)(2,1)S(1)} %shard_map.180), channel_id=1, source_target_pairs={{0,1},{1,0},{2,3},{3,2},{4,5},{5,4},{6,7},{7,6},{8,9},{9,8},{10,11... | collective-permute-start | bytes 393224 | tf_op jit(solution)/shard_map/ppermute | solution.py:479
  80.3 3.2 %collective-permute-start.3 = (bf16[128,512]{1,0:T(8,128)(2,1)S(1)}, bf16[128,512]{1,0:T(8,128)(2,1)S(1)}, u32[]{:S(2)}, u32[]{:S(2)}) collective-permute-start(bf16[128,512]{1,0:T(8,128)(2,1)S(1)} %shard_map.178), channel_id=1, source_target_pairs={{0,1},{1,0},{2,3},{3,2},{4,5},{5,4},{6,7},{7,6},{8,9},{9,8},{10,11... | collective-permute-start | bytes 393224 | tf_op jit(solution)/shard_map/ppermute | solution.py:476

commit v5 on v4

--- a/solution.py
+++ b/solution.py
@@ -1,4 +1,5 @@
 import functools
+import itertools
 
 import jax
 import jax.numpy as jnp
@@ -18,6 +19,8 @@
 PAD = 8
 RIM = 4
 HEAD = 16
+SLOTS = 8
+LOG2E = 1.4426950408889634
 FIRST_OUT = 52
 FIRST_BACK = 60
 
@@ -52,7 +55,7 @@
 
 
 def silu(v):
-    return v / (1.0 + jnp.exp(-v))
+    return v / (1.0 + jnp.exp2(v * -LOG2E))
 
 
 def pair_lanes(cols, q, rows):
@@ -84,7 +87,8 @@
     return copies
 
 
-def filtered(rows, taps, rim, pad_ref):
+def filtered(rows, taps, rim, pads):
+    pad_ref = next(pads)
     length, width = rows.shape
     span = taps.shape[0]
     if rim is None:
@@ -112,8 +116,9 @@
     weighted_ref, writes_ref, reads_ref, inside_ref, conv_ref, open_ref, head_ref,
     xt_ref, wt_ref, rt_ref, ct_ref, scale_ref, dt_ref, rise_ref, remain_ref, both_ref, rim_ref,
     x_ref, w_ref, r_ref, i_ref, v_ref, o_ref, gate_ref,
-    step_ref, spike_ref, off_ref, rate_ref, pad_ref, sems,
+    step_ref, spike_ref, off_ref, rate_ref, rises_ref, wide_ref, left_ref, pad_ref, sems,
 ):
+    pads = itertools.cycle([pad_ref.at[k] for k in range(SLOTS)])
     width = x_hbm.shape[2]
     narrow = w_hbm.shape[2]
     broad = i_hbm.shape[2]
@@ -148,9 +153,12 @@
     fall_t = spike_ref[...] - dt_t * column(jnp.exp(rate_ref[...]))
     row = lax.broadcasted_iota(jnp.int32, (length, length), 0)
     col = lax.broadcasted_iota(jnp.int32, (length, length), 1)
-    rise_t = jnp.dot(
-        fall_t, (row <= col).astype(F32), precision=lax.Precision.HIGHEST, preferred_element_type=F32
-    )
+    high = fall_t.astype(BF16)
+    rest = fall_t - high.astype(F32)
+    middle = rest.astype(BF16)
+    parts = jnp.concatenate([high, middle, (rest - middle.astype(F32)).astype(BF16)], axis=0)
+    sums = jnp.dot(parts, (row <= col).astype(BF16), preferred_element_type=F32)
+    rise_t = sums[0:heads] + sums[heads : 2 * heads] + sums[2 * heads :]
     tall = jnp.concatenate([rise_t, dt_t, jnp.zeros((LANES - 2 * heads, length), F32)], axis=0)
     turned_over = jnp.transpose(tall)
     rise = turned_over[:, 0:heads]
@@ -163,14 +171,18 @@
         copy.wait()
     groups = narrow // STATE
     per_group = width // LANES // groups
+    rise2_t = rise_t * LOG2E
+    rises_ref[...] = spread(three(rise * LOG2E), 0, LANES, heads * LANES)
+    wide_ref[...] = spread(three(dt), 0, HEAD_DIM, width)
+    left_ref[...] = spread(three(dt * remain), 0, HEAD_DIM, width)
     scores = []
     for g in range(groups):
         cols = slice(g * STATE, (g + 1) * STATE)
         write = silu(
-            filtered(w_ref[:, cols].astype(F32), wt_ref[:, cols].astype(F32), None, pad_ref)
+            filtered(w_ref[:, cols].astype(F32), wt_ref[:, cols].astype(F32), None, pads)
         ).astype(BF16)
         read = silu(
-            filtered(r_ref[:, cols].astype(F32), rt_ref[:, cols].astype(F32), None, pad_ref)
+            filtered(r_ref[:, cols].astype(F32), rt_ref[:, cols].astype(F32), None, pads)
         ).astype(BF16)
         writes_ref[:, cols] = write
         reads_ref[:, cols] = read
@@ -182,9 +194,9 @@
     late = lax.broadcasted_iota(jnp.int32, (length, LANES), 0) >= HEAD
     for q in range(width // LANES):
         cols = slice(q * LANES, (q + 1) * LANES)
-        x = silu(filtered(x_ref[:, cols].astype(F32), xt_ref[:, cols].astype(F32), None, pad_ref))
-        x = x * pair_lanes(dt, q, length)
-        weighted_ref[:, cols] = (x * pair_lanes(remain, q, length)).astype(BF16)
+        x = silu(filtered(x_ref[:, cols].astype(F32), xt_ref[:, cols].astype(F32), None, pads))
+        weighted_ref[:, cols] = (x * left_ref[:, cols]).astype(BF16)
+        x = x * wide_ref[:, cols]
         stacked = jnp.concatenate(
             [
                 jnp.where(low & late, x, 0.0).astype(BF16),
@@ -193,9 +205,10 @@
             axis=0,
         )
         both = []
-        for h in (2 * q, 2 * q + 1):
-            gap = jnp.minimum(rise[:, h : h + 1] - rise_t[h : h + 1, :], 0.0)
-            both.append((scores[q // per_group] * jnp.exp(gap)).astype(BF16))
+        for k in range(2):
+            h = 2 * q + k
+            gap = jnp.minimum(rises_ref[:, h * LANES : (h + 1) * LANES] - rise2_t[h : h + 1, :], 0.0)
+            both.append((scores[q // per_group] * jnp.exp2(gap)).astype(BF16))
         inside_ref[:, cols] = jnp.dot(
             jnp.concatenate(both, axis=1), stacked, preferred_element_type=F32
         )
@@ -206,7 +219,7 @@
     for c in range(0, broad, LANES):
         cols = slice(c, c + LANES)
         product = i_ref[:, cols].astype(F32) * v_ref[:, cols].astype(F32)
-        total = filtered(product, ct_ref[:, cols].astype(F32), None, pad_ref)
+        total = filtered(product, ct_ref[:, cols].astype(F32), None, pads)
         conv_ref[:, cols] = (o_ref[:, cols].astype(F32) * total).astype(BF16)
     at = 0
     for ref in (x_ref, w_ref, r_ref, i_ref, v_ref, o_ref):
@@ -221,6 +234,7 @@
     xt_ref, wt_ref, rt_ref, ct_ref, dt_ref, rise_ref, remain_ref,
     pay_ref, reads_ref, inside_ref, conv_ref, pad_ref,
 ):
+    pads = itertools.cycle([pad_ref.at[k] for k in range(SLOTS)])
     length, width = weighted_ref.shape
     heads = rise_ref.shape[1]
     narrow = writes_ref.shape[1]
@@ -240,13 +254,14 @@
                 head_ref[:, spot].astype(F32),
                 taps_ref[:, cols].astype(F32),
                 rim_ref[:, spot].astype(F32),
-                pad_ref,
+                pads,
             )
         )
 
     lane = lax.broadcasted_iota(jnp.int32, (length, LANES), 1)
     row = lax.broadcasted_iota(jnp.int32, (length, LANES), 0)
     share = heads // groups
+    rise_parts = three(rise)
     for g in range(groups):
         cols = slice(g * STATE, (g + 1) * STATE)
         spot = slice(width + g * STATE, width + (g + 1) * STATE)
@@ -275,21 +290,17 @@
             read, jnp.concatenate([first_write] * share, axis=0), (((1,), (1,)), ((), ())),
             preferred_element_type=F32,
         )
-        spread = (
-            lax.broadcasted_iota(jnp.int32, (heads, LANES), 0)
-            == g * share + lax.broadcasted_iota(jnp.int32, (heads, LANES), 1) // HEAD
-        ).astype(F32)
-        rises = jnp.dot(rise, spread, precision=lax.Precision.HIGHEST, preferred_element_type=F32)
-        here = (row == lane % HEAD)[0:HEAD]
+        rises = spread(rise_parts, g * share, HEAD, LANES)
+        here = (row == (lane & (HEAD - 1)))[0:HEAD]
         start = jnp.sum(jnp.where(here, rises[0:HEAD], 0.0), axis=0, keepdims=True)
         kept = jnp.where(
-            lane % HEAD <= row, scores * jnp.exp(jnp.minimum(rises - start, 0.0)), 0.0
+            (lane & (HEAD - 1)) <= row, scores * jnp.exp(jnp.minimum(rises - start, 0.0)), 0.0
         ).astype(BF16)
         span = per_group * LANES
         tiled = jnp.concatenate([jnp.concatenate(firsts, axis=1)] * share, axis=0)
         own = (
-            lax.broadcasted_iota(jnp.int32, (LANES, span), 0) // HEAD
-            == lax.broadcasted_iota(jnp.int32, (LANES, span), 1) // HEAD_DIM
+            lax.broadcasted_iota(jnp.int32, (LANES, span), 0) >> (HEAD.bit_length() - 1)
+            == lax.broadcasted_iota(jnp.int32, (LANES, span), 1) >> (HEAD_DIM.bit_length() - 1)
         )
         tiled = jnp.where(own, tiled, jnp.zeros_like(tiled))
         wide = slice(g * span, (g + 1) * span)
@@ -302,7 +313,7 @@
         o = slice(base + 2 * broad + c, base + 2 * broad + c + LANES)
         product = head_ref[:, i].astype(F32) * head_ref[:, v].astype(F32)
         rim = rim_ref[:, i].astype(F32) * rim_ref[:, v].astype(F32)
-        value = filtered(product, ct_ref[:, cols].astype(F32), rim, pad_ref)
+        value = filtered(product, ct_ref[:, cols].astype(F32), rim, pads)
         conv_ref[0:HEAD, cols] = (head_ref[:, o].astype(F32) * value).astype(BF16)
         conv_ref[HEAD:, cols] = conv_in[HEAD:, cols]
 
@@ -437,12 +448,15 @@
         sds((1, width), F32), sds((HEAD, heads), F32), sds((length, heads), F32), sds((HEAD, heads), F32),
         sds((width + wide, state_output_rows.shape[1]), BF16), sds((RIM, all_width), BF16),
     ]
-    pad = vmem((PAD + length, LANES))
+    pad = vmem((SLOTS, PAD + length, LANES))
     scratch = [vmem(a.shape[1:], BF16) for a in ins[:7]] + [
         vmem((heads, length)),
         vmem((heads, length)),
         vmem((1, heads)),
         vmem((1, heads)),
+        vmem((length, heads * LANES)),
+        vmem((length, width)),
+        vmem((length, width)),
         pad,
         sems(18),
     ]

time: 84.7 us -> 84.3 us (level)
  no operation moved by 1% of the time
where the time goes in v5:
time: 84.3 us; the launch traced here: 83.9 us
  blocking collectives  45.7 us (54%)
  starting transfers between devices  26.9 us (32%)
  Pallas kernels  6.43 us (8%)
  waiting for transfers between devices  4.73 us (6%)
    all_to_all x1, blocking collectives, per_device(): lax.all_to_all(payload, 'sp', 0, 0, axis_index_groups=turned(members, FIR...  28 us
    all_to_all x1, blocking collectives, per_device(): lax.all_to_all(prefixes, 'sp', 0, 0, axis_index_groups=turned(members, FI...  17.7 us
    ppermute x4, starting transfers between devices, moved(): lax.ppermute(value, 'fs', [(k, (k + away) % seqs) for k in range(seqs)])  13.1 us
    ppermute x1, starting transfers between devices, per_device(): late_got = lax.ppermute(sent, 'tp', swap)  7.87 us
    pallas_call x10, Pallas kernels, call(): pl.pallas_call(kernel, grid=(1,), in_specs=[HBM] * far + [whole(a.shape)...  6.43 us
    ppermute x1, starting transfers between devices, per_device(): before = lax.ppermute(rims, 'sp', [(k, k + 1) for k in range(members - 1)])  4.02 us
    ppermute x4, waiting for transfers between devices, moved(): lax.ppermute(value, 'fs', [(k, (k + away) % seqs) for k in range(seqs)])  3.87 us
    ppermute x1, starting transfers between devices, per_device(): early_got = lax.ppermute(sent, 'tp', swap)  1.92 us
  transfers between devices with their start and end apart: 7, of which 3 were waited for; matrix products, arithmetic and copies ran while one was open for 0% of the time, Pallas kernels for 4%

profile of v5, /device:TPU:1, one launch (start us, length us, event | category | flops | bytes accessed | tf_op | source)
XLA Modules:
  0.0 83.9 jit_solution(3340528224062557891)
XLA Ops:
  0.0 2.7 %shard_map.172 = (bf16[128,1024]{1,0:T(8,128)(2,1)S(1)}, bf16[128,256]{1,0:T(8,128)(2,1)S(1)}, bf16[128,256]{1,0:T(8,128)(2,1)S(1)}, f32[128,1024]{1,0:T(8,128)S...) custom-call(bf16[1,128,1024]{2,1,0:T(8,128)(2,1)} %x_hbm.1, ...), custom_call_target="tpu_custom_call" | custom-call | flops 50000000 | bytes 2000000 | tf_op jit(solution)/shard_map/pallas_call | solution.py:37
  2.7 4.0 %collective-permute-start = (bf16[4,2560]{1,0:T(4,128)(2,1)S(1)}, bf16[4,2560]{1,0:T(4,128)(2,1)S(1)}, u32[]{:S(2)}, u32[]{:S(2)}) collective-permute-start(bf16[4,2560]{1,0:T(4,128)(2,1)S(1)} %get-tuple-element.26), channel_id=1, source_target_pairs={{0,8},{8,16},{16,24},{24,32},{32,40},{40,48},{48,56},{56,64},{64,7... | collective-permute-start | bytes 61448 | tf_op jit(solution)/shard_map/ppermute | solution.py:467
  6.7 4.7 %collective-permute-start.1 = (bf16[1536,512]{1,0:T(8,128)(2,1)S(1)}, bf16[1536,512]{1,0:T(8,128)(2,1)S(1)}, u32[]{:S(2)}, u32[]{:S(2)}) collective-permute-start(bf16[1536,512]{1,0:T(8,128)(2,1)S(1)} %get-tuple-element.46.w_ref), channel_id=1, source_target_pairs={{0,4},{2,6},{4,0},{6,2},{1,5},{3,7},{5,1},{7,3},{8,12},{10,14},{12... | collective-permute-start | bytes 4718600 | tf_op jit(solution)/shard_map/ppermute | solution.py:474
  11.4 0.0 collective-permute-done.rim_ref
  11.4 0.8 shard_map.173
  12.2 28.0 %all_to_all.10.in_ref = bf16[64,24,128]{2,1,0:T(8,128)(2,1)S(1)} all-to-all(bf16[64,24,128]{2,1,0:T(8,128)(2,1)S(1)} %get-tuple-element.40), channel_id=1, replica_groups={{416,424,432,440,448,456,464,472,480,488,496,504,0,8,16,24,32,40,48,56,..., dimensions={0} | all-to-all | bytes 786432 | tf_op jit(solution)/shard_map/all_to_all | solution.py:477
  40.2 0.1 shard_map.174
  40.3 17.7 %all_to_all.11.p_ref = bf16[64,16,128]{2,1,0:T(8,128)(2,1)S(1)} all-to-all(bf16[64,16,128]{2,1,0:T(8,128)(2,1)S(1)} %shard_map.174), channel_id=1, replica_groups={{480,488,496,504,0,8,16,24,32,40,48,56,64,72,80,88,96,104,112,120,128,1..., dimensions={0} | all-to-all | bytes 524288 | tf_op jit(solution)/shard_map/all_to_all | solution.py:481
  58.1 0.5 shard_map.175.a_ref.first_ref
  58.6 2.2 %collective-permute-start.5 = (bf16[128,1536]{1,0:T(8,128)(2,1)S(1)}, bf16[128,1536]{1,0:T(8,128)(2,1)S(1)}, u32[]{:S(2)}, u32[]{:S(2)}) collective-permute-start(bf16[128,1536]{1,0:T(8,128)(2,1)S(1)} %shard_map.175.a_ref.first_ref), channel_id=1, source_target_pairs={{0,2},{2,4},{4,6},{6,0},{1,3},{3,5},{5,7},{7,1},{8,10},{10,12},{12... | collective-permute-start | bytes 1179656 | tf_op jit(solution)/shard_map/ppermute | solution.py:474
  60.8 4.3 %collective-permute-start.4 = (bf16[128,1536]{1,0:T(8,128)(2,1)S(1)}, bf16[128,1536]{1,0:T(8,128)(2,1)S(1)}, u32[]{:S(2)}, u32[]{:S(2)}) collective-permute-start(bf16[128,1536]{1,0:T(8,128)(2,1)S(1)} %shard_map.175.a_ref.first_ref), channel_id=1, source_target_pairs={{0,6},{2,0},{4,2},{6,4},{1,7},{3,1},{5,3},{7,5},{8,14},{10,8},{12,... | collective-permute-start | bytes 1179656 | tf_op jit(solution)/shard_map/ppermute | solution.py:474
  65.1 0.0 collective-permute-done.1.w_ref
  65.1 0.4 shard_map.176
  65.5 1.9 %collective-permute-start.2 = (bf16[128,512]{1,0:T(8,128)(2,1)S(1)}, bf16[128,512]{1,0:T(8,128)(2,1)S(1)}, u32[]{:S(2)}, u32[]{:S(2)}) collective-permute-start(bf16[128,512]{1,0:T(8,128)(2,1)S(1)} %shard_map.176), channel_id=1, source_target_pairs={{0,4},{2,6},{4,0},{6,2},{1,5},{3,7},{5,1},{7,3},{8,12},{10,14},{12... | collective-permute-start | bytes 393224 | tf_op jit(solution)/shard_map/ppermute | solution.py:474
  67.4 1.8 %collective-permute-done.5.second_ref = bf16[128,1536]{1,0:T(8,128)(2,1)S(1)} collective-permute-done((bf16[128,1536]{1,0:T(8,128)(2,1)S(1)}, bf16[128,1536]{1,0:T(8,128)(2,1)S(1)}, u32[]{:S(2)}, u32[]{:S(2)}) %collective-permute-start.5) | collective-permute-done | bytes 393248 | tf_op jit(solution)/shard_map/ppermute | solution.py:474
  69.2 2.1 %collective-permute-done.4.first_ref = bf16[128,1536]{1,0:T(8,128)(2,1)S(1)} collective-permute-done((bf16[128,1536]{1,0:T(8,128)(2,1)S(1)}, bf16[128,1536]{1,0:T(8,128)(2,1)S(1)}, u32[]{:S(2)}, u32[]{:S(2)}) %collective-permute-start.4) | collective-permute-done | bytes 393248 | tf_op jit(solution)/shard_map/ppermute | solution.py:474
  71.3 0.4 shard_map.180
  71.6 7.9 %collective-permute-start.6 = (bf16[128,512]{1,0:T(8,128)(2,1)S(1)}, bf16[128,512]{1,0:T(8,128)(2,1)S(1)}, u32[]{:S(2)}, u32[]{:S(2)}) collective-permute-start(bf16[128,512]{1,0:T(8,128)(2,1)S(1)} %shard_map.180), channel_id=1, source_target_pairs={{0,1},{1,0},{2,3},{3,2},{4,5},{5,4},{6,7},{7,6},{8,9},{9,8},{10,11... | collective-permute-start | bytes 393224 | tf_op jit(solution)/shard_map/ppermute | solution.py:493
  79.5 0.0 collective-permute-done.2.second_ref
  79.5 0.4 shard_map.178
  79.9 1.9 %collective-permute-start.3 = (bf16[128,512]{1,0:T(8,128)(2,1)S(1)}, bf16[128,512]{1,0:T(8,128)(2,1)S(1)}, u32[]{:S(2)}, u32[]{:S(2)}) collective-permute-start(bf16[128,512]{1,0:T(8,128)(2,1)S(1)} %shard_map.178), channel_id=1, source_target_pairs={{0,1},{1,0},{2,3},{3,2},{4,5},{5,4},{6,7},{7,6},{8,9},{9,8},{10,11... | collective-permute-start | bytes 393224 | tf_op jit(solution)/shard_map/ppermute | solution.py:490
  81.9 0.4 shard_map.179.late_ref
  82.3 0.0 collective-permute-done.6.late_got_ref
  82.3 0.9 %collective-permute-done.3.early_got_ref = bf16[128,512]{1,0:T(8,128)(2,1)S(1)} collective-permute-done((bf16[128,512]{1,0:T(8,128)(2,1)S(1)}, bf16[128,512]{1,0:T(8,128)(2,1)S(1)}, u32[]{:S(2)}, u32[]{:S(2)}) %collective-permute-start.3) | collective-permute-done | bytes 131104 | tf_op jit(solution)/shard_map/ppermute | solution.py:490
  83.2 0.7 shard_map.181
  (1 shorter events, 0.0 us)
Async XLA Ops:
  2.7 8.7 %collective-permute-start = (bf16[4,2560]{1,0:T(4,128)(2,1)S(1)}, bf16[4,2560]{1,0:T(4,128)(2,1)S(1)}, u32[]{:S(2)}, u32[]{:S(2)}) collective-permute-start(bf16[4,2560]{1,0:T(4,128)(2,1)S(1)} %get-tuple-element.26), channel_id=1, source_target_pairs={{0,8},{8,16},{16,24},{24,32},{32,40},{40,48},{48,56},{56,64},{64,7... | collective-permute-start | bytes 61448 | tf_op jit(solution)/shard_map/ppermute | solution.py:467
  6.7 58.3 %collective-permute-start.1 = (bf16[1536,512]{1,0:T(8,128)(2,1)S(1)}, bf16[1536,512]{1,0:T(8,128)(2,1)S(1)}, u32[]{:S(2)}, u32[]{:S(2)}) collective-permute-start(bf16[1536,512]{1,0:T(8,128)(2,1)S(1)} %get-tuple-element.46.w_ref), channel_id=1, source_target_pairs={{0,4},{2,6},{4,0},{6,2},{1,5},{3,7},{5,1},{7,3},{8,12},{10,14},{12... | collective-permute-start | bytes 4718600 | tf_op jit(solution)/shard_map/ppermute | solution.py:474
  58.6 10.6 %collective-permute-start.5 = (bf16[128,1536]{1,0:T(8,128)(2,1)S(1)}, bf16[128,1536]{1,0:T(8,128)(2,1)S(1)}, u32[]{:S(2)}, u32[]{:S(2)}) collective-permute-start(bf16[128,1536]{1,0:T(8,128)(2,1)S(1)} %shard_map.175.a_ref.first_ref), channel_id=1, source_target_pairs={{0,2},{2,4},{4,6},{6,0},{1,3},{3,5},{5,7},{7,1},{8,10},{10,12},{12... | collective-permute-start | bytes 1179656 | tf_op jit(solution)/shard_map/ppermute | solution.py:474
  60.8 10.5 %collective-permute-start.4 = (bf16[128,1536]{1,0:T(8,128)(2,1)S(1)}, bf16[128,1536]{1,0:T(8,128)(2,1)S(1)}, u32[]{:S(2)}, u32[]{:S(2)}) collective-permute-start(bf16[128,1536]{1,0:T(8,128)(2,1)S(1)} %shard_map.175.a_ref.first_ref), channel_id=1, source_target_pairs={{0,6},{2,0},{4,2},{6,4},{1,7},{3,1},{5,3},{7,5},{8,14},{10,8},{12,... | collective-permute-start | bytes 1179656 | tf_op jit(solution)/shard_map/ppermute | solution.py:474
  65.5 14.1 %collective-permute-start.2 = (bf16[128,512]{1,0:T(8,128)(2,1)S(1)}, bf16[128,512]{1,0:T(8,128)(2,1)S(1)}, u32[]{:S(2)}, u32[]{:S(2)}) collective-permute-start(bf16[128,512]{1,0:T(8,128)(2,1)S(1)} %shard_map.176), channel_id=1, source_target_pairs={{0,4},{2,6},{4,0},{6,2},{1,5},{3,7},{5,1},{7,3},{8,12},{10,14},{12... | collective-permute-start | bytes 393224 | tf_op jit(solution)/shard_map/ppermute | solution.py:474
  71.6 10.7 %collective-permute-start.6 = (bf16[128,512]{1,0:T(8,128)(2,1)S(1)}, bf16[128,512]{1,0:T(8,128)(2,1)S(1)}, u32[]{:S(2)}, u32[]{:S(2)}) collective-permute-start(bf16[128,512]{1,0:T(8,128)(2,1)S(1)} %shard_map.180), channel_id=1, source_target_pairs={{0,1},{1,0},{2,3},{3,2},{4,5},{5,4},{6,7},{7,6},{8,9},{9,8},{10,11... | collective-permute-start | bytes 393224 | tf_op jit(solution)/shard_map/ppermute | solution.py:493
  79.9 3.2 %collective-permute-start.3 = (bf16[128,512]{1,0:T(8,128)(2,1)S(1)}, bf16[128,512]{1,0:T(8,128)(2,1)S(1)}, u32[]{:S(2)}, u32[]{:S(2)}) collective-permute-start(bf16[128,512]{1,0:T(8,128)(2,1)S(1)} %shard_map.178), channel_id=1, source_target_pairs={{0,1},{1,0},{2,3},{3,2},{4,5},{5,4},{6,7},{7,6},{8,9},{9,8},{10,11... | collective-permute-start | bytes 393224 | tf_op jit(solution)/shard_map/ppermute | solution.py:490

commit v6 on v5

--- a/solution.py
+++ b/solution.py
@@ -334,11 +334,11 @@
             carry = carry * decay + in_ref[at, 0:16, :].astype(F32)
 
 
-def gate_kernel(p_ref, reads_ref, rise_ref, inside_ref, open_ref, scale_ref, conv_ref, out_ref):
+def gate_kernel(p_ref, reads_ref, rise_ref, inside_ref, open_ref, scale_ref, conv_ref, out_ref, kept_ref):
     length, width = inside_ref.shape
     groups = reads_ref.shape[1] // STATE
     per_group = width // LANES // groups
-    kept = three(jnp.exp(rise_ref[...]))
+    kept_ref[...] = spread(three(jnp.exp(rise_ref[...])), 0, HEAD_DIM, width)
     blocks = STATE // 16
     for g in range(groups):
         read = reads_ref[:, g * STATE : (g + 1) * STATE]
@@ -349,7 +349,7 @@
             spots = [(q * blocks + k + FIRST_OUT - FIRST_BACK) % p_ref.shape[0] for k in range(blocks)]
             before = jnp.concatenate([p_ref[spot] for spot in spots], axis=0)
             carried = jnp.dot(read, before, preferred_element_type=F32)
-            y = inside_ref[:, cols] + carried * spread(kept, 2 * q, HEAD_DIM, LANES)
+            y = inside_ref[:, cols] + carried * kept_ref[:, cols]
             y = y * open_ref[:, cols]
             squares = squares + y * y
             gated.append(y)
@@ -480,7 +480,7 @@
     prefixes = call(scan_kernel, [sds((members, 16, LANES), BF16)], (gathered,))[0]
     incoming = lax.all_to_all(prefixes, "sp", 0, 0, axis_index_groups=turned(members, FIRST_BACK), tiled=True)
     ins = (incoming, reads, rise, inside, opened, scale, conv)
-    own = call(gate_kernel, [sds((length, width + wide), BF16)], ins)[0]
+    own = call(gate_kernel, [sds((length, width + wide), BF16)], ins, 0, [vmem((length, width))])[0]
     last = moved(own, 1)
     following = moved(own, -1)
     partial = call(far_kernel, [sds((length, rows_own.shape[1]), BF16)], (own, rows_far))[0]

time: 84.3 us -> 84.4 us (level)
  no operation moved by 1% of the time
where the time goes in v6:
time: 84.4 us; the launch traced here: 83.9 us
  blocking collectives  45.7 us (54%)
  starting transfers between devices  26.9 us (32%)
  Pallas kernels  6.44 us (8%)
  waiting for transfers between devices  4.71 us (6%)
    all_to_all x1, blocking collectives, per_device(): lax.all_to_all(payload, 'sp', 0, 0, axis_index_groups=turned(members, FIR...  28 us
    all_to_all x1, blocking collectives, per_device(): lax.all_to_all(prefixes, 'sp', 0, 0, axis_index_groups=turned(members, FI...  17.7 us
    ppermute x4, starting transfers between devices, moved(): lax.ppermute(value, 'fs', [(k, (k + away) % seqs) for k in range(seqs)])  13.1 us
    ppermute x1, starting transfers between devices, per_device(): late_got = lax.ppermute(sent, 'tp', swap)  7.89 us
    pallas_call x10, Pallas kernels, call(): pl.pallas_call(kernel, grid=(1,), in_specs=[HBM] * far + [whole(a.shape)...  6.44 us
    ppermute x1, starting transfers between devices, per_device(): before = lax.ppermute(rims, 'sp', [(k, k + 1) for k in range(members - 1)])  4.02 us
    ppermute x4, waiting for transfers between devices, moved(): lax.ppermute(value, 'fs', [(k, (k + away) % seqs) for k in range(seqs)])  3.85 us
    ppermute x1, starting transfers between devices, per_device(): early_got = lax.ppermute(sent, 'tp', swap)  1.92 us
  transfers between devices with their start and end apart: 7, of which 3 were waited for; matrix products, arithmetic and copies ran while one was open for 0% of the time, Pallas kernels for 4%

profile of v6, /device:TPU:1, one launch (start us, length us, event | category | flops | bytes accessed | tf_op | source)
XLA Modules:
  0.0 83.9 jit_solution(10919632741185815541)
XLA Ops:
  0.0 2.7 %shard_map.172 = (bf16[128,1024]{1,0:T(8,128)(2,1)S(1)}, bf16[128,256]{1,0:T(8,128)(2,1)S(1)}, bf16[128,256]{1,0:T(8,128)(2,1)S(1)}, f32[128,1024]{1,0:T(8,128)S...) custom-call(bf16[1,128,1024]{2,1,0:T(8,128)(2,1)} %x_hbm.1, ...), custom_call_target="tpu_custom_call" | custom-call | flops 50000000 | bytes 2000000 | tf_op jit(solution)/shard_map/pallas_call | solution.py:37
  2.7 4.0 %collective-permute-start = (bf16[4,2560]{1,0:T(4,128)(2,1)S(1)}, bf16[4,2560]{1,0:T(4,128)(2,1)S(1)}, u32[]{:S(2)}, u32[]{:S(2)}) collective-permute-start(bf16[4,2560]{1,0:T(4,128)(2,1)S(1)} %get-tuple-element.26), channel_id=1, source_target_pairs={{0,8},{8,16},{16,24},{24,32},{32,40},{40,48},{48,56},{56,64},{64,7... | collective-permute-start | bytes 61448 | tf_op jit(solution)/shard_map/ppermute | solution.py:467
  6.7 4.7 %collective-permute-start.1 = (bf16[1536,512]{1,0:T(8,128)(2,1)S(1)}, bf16[1536,512]{1,0:T(8,128)(2,1)S(1)}, u32[]{:S(2)}, u32[]{:S(2)}) collective-permute-start(bf16[1536,512]{1,0:T(8,128)(2,1)S(1)} %get-tuple-element.46.w_ref), channel_id=1, source_target_pairs={{0,4},{2,6},{4,0},{6,2},{1,5},{3,7},{5,1},{7,3},{8,12},{10,14},{12... | collective-permute-start | bytes 4718600 | tf_op jit(solution)/shard_map/ppermute | solution.py:474
  11.4 0.0 collective-permute-done.rim_ref
  11.4 0.8 shard_map.173
  12.2 28.0 %all_to_all.10.in_ref = bf16[64,24,128]{2,1,0:T(8,128)(2,1)S(1)} all-to-all(bf16[64,24,128]{2,1,0:T(8,128)(2,1)S(1)} %get-tuple-element.40), channel_id=1, replica_groups={{416,424,432,440,448,456,464,472,480,488,496,504,0,8,16,24,32,40,48,56,..., dimensions={0} | all-to-all | bytes 786432 | tf_op jit(solution)/shard_map/all_to_all | solution.py:477
  40.2 0.1 shard_map.174
  40.3 17.7 %all_to_all.11.p_ref = bf16[64,16,128]{2,1,0:T(8,128)(2,1)S(1)} all-to-all(bf16[64,16,128]{2,1,0:T(8,128)(2,1)S(1)} %shard_map.174), channel_id=1, replica_groups={{480,488,496,504,0,8,16,24,32,40,48,56,64,72,80,88,96,104,112,120,128,1..., dimensions={0} | all-to-all | bytes 524288 | tf_op jit(solution)/shard_map/all_to_all | solution.py:481
  58.1 0.5 shard_map.175.a_ref.first_ref
  58.6 2.2 %collective-permute-start.5 = (bf16[128,1536]{1,0:T(8,128)(2,1)S(1)}, bf16[128,1536]{1,0:T(8,128)(2,1)S(1)}, u32[]{:S(2)}, u32[]{:S(2)}) collective-permute-start(bf16[128,1536]{1,0:T(8,128)(2,1)S(1)} %shard_map.175.a_ref.first_ref), channel_id=1, source_target_pairs={{0,2},{2,4},{4,6},{6,0},{1,3},{3,5},{5,7},{7,1},{8,10},{10,12},{12... | collective-permute-start | bytes 1179656 | tf_op jit(solution)/shard_map/ppermute | solution.py:474
  60.8 4.3 %collective-permute-start.4 = (bf16[128,1536]{1,0:T(8,128)(2,1)S(1)}, bf16[128,1536]{1,0:T(8,128)(2,1)S(1)}, u32[]{:S(2)}, u32[]{:S(2)}) collective-permute-start(bf16[128,1536]{1,0:T(8,128)(2,1)S(1)} %shard_map.175.a_ref.first_ref), channel_id=1, source_target_pairs={{0,6},{2,0},{4,2},{6,4},{1,7},{3,1},{5,3},{7,5},{8,14},{10,8},{12,... | collective-permute-start | bytes 1179656 | tf_op jit(solution)/shard_map/ppermute | solution.py:474
  65.1 0.0 collective-permute-done.1.w_ref
  65.1 0.4 shard_map.176
  65.5 1.9 %collective-permute-start.2 = (bf16[128,512]{1,0:T(8,128)(2,1)S(1)}, bf16[128,512]{1,0:T(8,128)(2,1)S(1)}, u32[]{:S(2)}, u32[]{:S(2)}) collective-permute-start(bf16[128,512]{1,0:T(8,128)(2,1)S(1)} %shard_map.176), channel_id=1, source_target_pairs={{0,4},{2,6},{4,0},{6,2},{1,5},{3,7},{5,1},{7,3},{8,12},{10,14},{12... | collective-permute-start | bytes 393224 | tf_op jit(solution)/shard_map/ppermute | solution.py:474
  67.4 1.8 %collective-permute-done.5.second_ref = bf16[128,1536]{1,0:T(8,128)(2,1)S(1)} collective-permute-done((bf16[128,1536]{1,0:T(8,128)(2,1)S(1)}, bf16[128,1536]{1,0:T(8,128)(2,1)S(1)}, u32[]{:S(2)}, u32[]{:S(2)}) %collective-permute-start.5) | collective-permute-done | bytes 393248 | tf_op jit(solution)/shard_map/ppermute | solution.py:474
  69.2 2.0 %collective-permute-done.4.first_ref = bf16[128,1536]{1,0:T(8,128)(2,1)S(1)} collective-permute-done((bf16[128,1536]{1,0:T(8,128)(2,1)S(1)}, bf16[128,1536]{1,0:T(8,128)(2,1)S(1)}, u32[]{:S(2)}, u32[]{:S(2)}) %collective-permute-start.4) | collective-permute-done | bytes 393248 | tf_op jit(solution)/shard_map/ppermute | solution.py:474
  71.2 0.4 shard_map.180
  71.6 7.9 %collective-permute-start.6 = (bf16[128,512]{1,0:T(8,128)(2,1)S(1)}, bf16[128,512]{1,0:T(8,128)(2,1)S(1)}, u32[]{:S(2)}, u32[]{:S(2)}) collective-permute-start(bf16[128,512]{1,0:T(8,128)(2,1)S(1)} %shard_map.180), channel_id=1, source_target_pairs={{0,1},{1,0},{2,3},{3,2},{4,5},{5,4},{6,7},{7,6},{8,9},{9,8},{10,11... | collective-permute-start | bytes 393224 | tf_op jit(solution)/shard_map/ppermute | solution.py:493
  79.5 0.0 collective-permute-done.2.second_ref
  79.5 0.4 shard_map.178
  79.9 1.9 %collective-permute-start.3 = (bf16[128,512]{1,0:T(8,128)(2,1)S(1)}, bf16[128,512]{1,0:T(8,128)(2,1)S(1)}, u32[]{:S(2)}, u32[]{:S(2)}) collective-permute-start(bf16[128,512]{1,0:T(8,128)(2,1)S(1)} %shard_map.178), channel_id=1, source_target_pairs={{0,1},{1,0},{2,3},{3,2},{4,5},{5,4},{6,7},{7,6},{8,9},{9,8},{10,11... | collective-permute-start | bytes 393224 | tf_op jit(solution)/shard_map/ppermute | solution.py:490
  81.9 0.4 shard_map.179.late_ref
  82.3 0.0 collective-permute-done.6.late_got_ref
  82.3 0.9 %collective-permute-done.3.early_got_ref = bf16[128,512]{1,0:T(8,128)(2,1)S(1)} collective-permute-done((bf16[128,512]{1,0:T(8,128)(2,1)S(1)}, bf16[128,512]{1,0:T(8,128)(2,1)S(1)}, u32[]{:S(2)}, u32[]{:S(2)}) %collective-permute-start.3) | collective-permute-done | bytes 131104 | tf_op jit(solution)/shard_map/ppermute | solution.py:490
  83.2 0.7 shard_map.181
  (1 shorter events, 0.0 us)
Async XLA Ops:
  2.7 8.7 %collective-permute-start = (bf16[4,2560]{1,0:T(4,128)(2,1)S(1)}, bf16[4,2560]{1,0:T(4,128)(2,1)S(1)}, u32[]{:S(2)}, u32[]{:S(2)}) collective-permute-start(bf16[4,2560]{1,0:T(4,128)(2,1)S(1)} %get-tuple-element.26), channel_id=1, source_target_pairs={{0,8},{8,16},{16,24},{24,32},{32,40},{40,48},{48,56},{56,64},{64,7... | collective-permute-start | bytes 61448 | tf_op jit(solution)/shard_map/ppermute | solution.py:467
  6.7 58.3 %collective-permute-start.1 = (bf16[1536,512]{1,0:T(8,128)(2,1)S(1)}, bf16[1536,512]{1,0:T(8,128)(2,1)S(1)}, u32[]{:S(2)}, u32[]{:S(2)}) collective-permute-start(bf16[1536,512]{1,0:T(8,128)(2,1)S(1)} %get-tuple-element.46.w_ref), channel_id=1, source_target_pairs={{0,4},{2,6},{4,0},{6,2},{1,5},{3,7},{5,1},{7,3},{8,12},{10,14},{12... | collective-permute-start | bytes 4718600 | tf_op jit(solution)/shard_map/ppermute | solution.py:474
  58.6 10.6 %collective-permute-start.5 = (bf16[128,1536]{1,0:T(8,128)(2,1)S(1)}, bf16[128,1536]{1,0:T(8,128)(2,1)S(1)}, u32[]{:S(2)}, u32[]{:S(2)}) collective-permute-start(bf16[128,1536]{1,0:T(8,128)(2,1)S(1)} %shard_map.175.a_ref.first_ref), channel_id=1, source_target_pairs={{0,2},{2,4},{4,6},{6,0},{1,3},{3,5},{5,7},{7,1},{8,10},{10,12},{12... | collective-permute-start | bytes 1179656 | tf_op jit(solution)/shard_map/ppermute | solution.py:474
  60.8 10.4 %collective-permute-start.4 = (bf16[128,1536]{1,0:T(8,128)(2,1)S(1)}, bf16[128,1536]{1,0:T(8,128)(2,1)S(1)}, u32[]{:S(2)}, u32[]{:S(2)}) collective-permute-start(bf16[128,1536]{1,0:T(8,128)(2,1)S(1)} %shard_map.175.a_ref.first_ref), channel_id=1, source_target_pairs={{0,6},{2,0},{4,2},{6,4},{1,7},{3,1},{5,3},{7,5},{8,14},{10,8},{12,... | collective-permute-start | bytes 1179656 | tf_op jit(solution)/shard_map/ppermute | solution.py:474
  65.5 14.1 %collective-permute-start.2 = (bf16[128,512]{1,0:T(8,128)(2,1)S(1)}, bf16[128,512]{1,0:T(8,128)(2,1)S(1)}, u32[]{:S(2)}, u32[]{:S(2)}) collective-permute-start(bf16[128,512]{1,0:T(8,128)(2,1)S(1)} %shard_map.176), channel_id=1, source_target_pairs={{0,4},{2,6},{4,0},{6,2},{1,5},{3,7},{5,1},{7,3},{8,12},{10,14},{12... | collective-permute-start | bytes 393224 | tf_op jit(solution)/shard_map/ppermute | solution.py:474
  71.6 10.7 %collective-permute-start.6 = (bf16[128,512]{1,0:T(8,128)(2,1)S(1)}, bf16[128,512]{1,0:T(8,128)(2,1)S(1)}, u32[]{:S(2)}, u32[]{:S(2)}) collective-permute-start(bf16[128,512]{1,0:T(8,128)(2,1)S(1)} %shard_map.180), channel_id=1, source_target_pairs={{0,1},{1,0},{2,3},{3,2},{4,5},{5,4},{6,7},{7,6},{8,9},{9,8},{10,11... | collective-permute-start | bytes 393224 | tf_op jit(solution)/shard_map/ppermute | solution.py:493
  79.9 3.2 %collective-permute-start.3 = (bf16[128,512]{1,0:T(8,128)(2,1)S(1)}, bf16[128,512]{1,0:T(8,128)(2,1)S(1)}, u32[]{:S(2)}, u32[]{:S(2)}) collective-permute-start(bf16[128,512]{1,0:T(8,128)(2,1)S(1)} %shard_map.178), channel_id=1, source_target_pairs={{0,1},{1,0},{2,3},{3,2},{4,5},{5,4},{6,7},{7,6},{8,9},{9,8},{10,11... | collective-permute-start | bytes 393224 | tf_op jit(solution)/shard_map/ppermute | solution.py:490
